TPU v7x, 32 devices: a whole 2x2x4 slice. The times are simulated.
32 devices in a mesh: sp: 8 (over z, x), tp: 4 (over y, core).
Axes of the slice: x: 2, y: 2, z: 4, core: 2. Of those that a mesh axis runs over, the one named last changes fastest.
Arguments:
- residual: bfloat16 [3072, 2048], P('sp', 'tp'), may hold values from -6 to 6
- query_nope: bfloat16 [3072, 4096], P('sp', 'tp'), may hold values from -9 to 9
- query_rope: bfloat16 [3072, 2048], P('sp', 'tp'), may hold values from -600 to 600
- latent: bfloat16 [3072, 512], P('sp'), may hold values from -6 to 6
- rope_key: bfloat16 [3072, 64], P('sp'), may hold values from -6 to 6
- doc_ids: int32 [3072], P('sp'), may hold values from 0 to 3, never falling along the last dimension, each value on 1 to 1152 neighbouring positions
- key_up: bfloat16 [512, 4096], P(None, 'tp'), may hold values from -0.25 to 0.25
- value_up: bfloat16 [512, 4096], P(None, 'tp'), may hold values from -0.25 to 0.25
- out_proj: bfloat16 [4096, 2048], P('tp'), may hold values from -0.375 to 0.375
- norm1_gain: bfloat16 [2048], P('tp'), may hold values from 0.099609375 to 1.8984375
- norm1_bias: bfloat16 [2048], P('tp'), may hold values from -3 to 3
- ffn_gate: bfloat16 [2048, 5632], P('sp', 'tp'), may hold values from -0.125 to 0.125
- ffn_value: bfloat16 [2048, 5632], P('sp', 'tp'), may hold values from -0.125 to 0.125
- conv_gate: bfloat16 [3, 5632], P(None, 'tp'), may hold values from -3.5 to 3.5
- conv_value: bfloat16 [3, 5632], P(None, 'tp'), may hold values from -3.5 to 3.5
- ffn_down: bfloat16 [5632, 2048], P('tp', 'sp'), may hold values from -0.15625 to 0.15625
- norm2_gain: bfloat16 [2048], P('tp'), may hold values from 0.099609375 to 1.8984375
- norm2_bias: bfloat16 [2048], P('tp'), may hold values from -3 to 3
Outputs:
- layer_out: bfloat16 [3072, 2048], P('sp', 'tp')
Inputs may be any that keep to these rules, and one draw needn't show every extreme that they name: `doc_ids`: document numbers never fall along the positions; each document holds 1 to 1152 positions, and one holds exactly 1152.
All inputs are finite; a program needn't handle non-finite values.
Results may differ from a plain program's by a relative error of at most 0.014.
Values may be sent and summed in bfloat16 or wider, within the bound.
A program may use at most 128 MiB of HBM per device.

v0:
```python
import jax
import jax.numpy as jnp
from jax import lax
from jax.sharding import PartitionSpec as P

D = 2048
NOPE = 128
ROPE = 64
VDIM = 128
CONV = 3
REACH = 3


norm_eps = 1e-05
residual_scale = 8.0**0.25
rope_base_freq = 10000.0
masked_score = -1e30


def passed_along(value, axis, by):
    count = lax.axis_size(axis)
    pairs = [(i, i + by) for i in range(count) if 0 <= i + by < count]
    return lax.ppermute(value, axis, pairs)


def tables(positions):
    frequencies = 1.0 / rope_base_freq ** (jnp.arange(0, ROPE, 2, dtype=jnp.float32) / ROPE)
    angles = positions.astype(jnp.float32)[:, None] * frequencies[None, :]
    return (jnp.cos(angles), jnp.sin(angles))


def rotate(vectors, cosine, sine_table):
    half_width = vectors.shape[-1] // 2
    front_half = vectors[..., :half_width]
    back_half = vectors[..., half_width:]
    return jnp.concatenate(
        [
            front_half * cosine - back_half * sine_table,
            front_half * sine_table + back_half * cosine,
        ],
        axis=-1,
    )


def finish(mixed, totals, gain_row, bias_row):
    row_mean = totals[0][:, None] / D
    row_power = totals[1][:, None] / D
    return (mixed - row_mean) * lax.rsqrt(
        row_power - row_mean * row_mean + norm_eps
    ) * gain_row.astype(jnp.float32) + bias_row.astype(jnp.float32)


def local(
    residual,
    query_nope,
    query_rope,
    latent,
    rope_key,
    doc_ids,
    key_up,
    value_up,
    out_proj,
    norm1_gain,
    norm1_bias,
    ffn_gate,
    ffn_value,
    conv_gate,
    conv_value,
    ffn_down,
    norm2_gain,
    norm2_bias,
):
    row_count = latent.shape[0]
    head_count = query_nope.shape[1] // NOPE
    local_units = ffn_gate.shape[1]
    rim_rows = CONV - 1
    whole_gate, whole_value, whole_down = (
        lax.all_gather(ffn_gate, "sp", axis=0, tiled=True),
        lax.all_gather(ffn_value, "sp", axis=0, tiled=True),
        lax.all_gather(ffn_down, "sp", axis=1, tiled=True),
    )
    offset = lax.axis_index("sp") * row_count
    positions = offset + jnp.arange(row_count, dtype=jnp.int32)
    cosine, sine_table = tables(positions)
    turned_key = rotate(rope_key.astype(jnp.float32), cosine, sine_table).astype(jnp.bfloat16)
    turned_query = rotate(
        query_rope.astype(jnp.float32).reshape(row_count, head_count, ROPE),
        cosine[:, None],
        sine_table[:, None],
    ).astype(jnp.bfloat16)
    latent_list = []
    rim_list = []
    doc_list = []
    for shift_step in range(REACH, 0, -1):
        far_latent, far_key, far_doc = passed_along((latent, turned_key, doc_ids), "sp", shift_step)
        latent_list.append(far_latent)
        rim_list.append(far_key)
        doc_list.append(far_doc)
    win_latent = jnp.concatenate(latent_list + [latent], 0)
    win_key = jnp.concatenate(rim_list + [turned_key], 0)
    win_doc = jnp.concatenate(doc_list + [doc_ids], 0)
    key_rows = jnp.dot(win_latent, key_up, preferred_element_type=jnp.float32).astype(jnp.bfloat16)
    values = jnp.dot(win_latent, value_up, preferred_element_type=jnp.float32).astype(jnp.bfloat16)
    window = key_rows.shape[0]
    key_pos = offset - REACH * row_count + jnp.arange(window, dtype=jnp.int32)
    allowed = (
        (key_pos[None, :] <= positions[:, None])
        & (key_pos[None, :] >= 0)
        & (win_doc[None, :] == doc_ids[:, None])
    )
    scale = (NOPE + ROPE) ** (-0.5)
    scores = jnp.einsum(
        "qhd,khd->hqk",
        query_nope.reshape(row_count, head_count, NOPE),
        key_rows.reshape(window, head_count, NOPE),
        preferred_element_type=jnp.float32,
    )
    scores = scores + jnp.einsum(
        "qhr,kr->hqk", turned_query, win_key, preferred_element_type=jnp.float32
    )
    scores = jnp.where(allowed[None], scores * scale, masked_score)
    row_max = jnp.max(scores, -1, keepdims=True)
    weights = jnp.exp(scores - row_max)
    weights = (weights / jnp.sum(weights, -1, keepdims=True)).astype(jnp.bfloat16)
    attended = jnp.einsum(
        "hqk,khd->qhd",
        weights,
        values.reshape(window, head_count, VDIM),
        preferred_element_type=jnp.float32,
    )
    attended = attended.astype(jnp.bfloat16).reshape(row_count, head_count * VDIM)
    head_terms = jnp.dot(attended, out_proj, preferred_element_type=jnp.float32)
    projected = lax.psum_scatter(
        head_terms.astype(jnp.bfloat16), "tp", scatter_dimension=1, tiled=True
    ).astype(jnp.float32)
    mixed_one = residual_scale * residual.astype(jnp.float32) + projected
    totals_one = lax.psum((jnp.sum(mixed_one, 1), jnp.sum(mixed_one * mixed_one, 1)), "tp")
    normed = finish(mixed_one, totals_one, norm1_gain, norm1_bias).astype(jnp.bfloat16)
    full_rows = lax.all_gather(normed, "tp", axis=1, tiled=True)
    gate_sum = jnp.dot(full_rows, whole_gate, preferred_element_type=jnp.float32)
    value_sum = jnp.dot(full_rows, whole_value, preferred_element_type=jnp.float32)
    gate_pre = gate_sum.astype(jnp.bfloat16)
    value_pre = value_sum.astype(jnp.bfloat16)
    tail_gate, tail_value, tail_doc = passed_along(
        (
            gate_pre[row_count - rim_rows :],
            value_pre[row_count - rim_rows :],
            doc_ids[row_count - rim_rows :],
        ),
        "sp",
        1,
    )
    ext_gate = jnp.concatenate([tail_gate, gate_pre], 0)
    ext_value = jnp.concatenate([tail_value, value_pre], 0)
    ext_doc = jnp.concatenate([tail_doc, doc_ids], 0)
    gate_mix = jnp.zeros((row_count, local_units), jnp.float32)
    value_mix = jnp.zeros((row_count, local_units), jnp.float32)
    for tap_index in range(CONV):
        valid_tap = (
            (ext_doc[tap_index : tap_index + row_count] == doc_ids)
            & (positions - rim_rows + tap_index >= 0)
        ).astype(jnp.float32)[:, None]
        gate_mix = (
            gate_mix
            + conv_gate[tap_index].astype(jnp.float32)
            * ext_gate[tap_index : tap_index + row_count].astype(jnp.float32)
            * valid_tap
        )
        value_mix = (
            value_mix
            + conv_value[tap_index].astype(jnp.float32)
            * ext_value[tap_index : tap_index + row_count].astype(jnp.float32)
            * valid_tap
        )
    hidden = (value_mix * jax.nn.gelu(gate_mix)).astype(jnp.bfloat16)
    unit_terms = jnp.dot(hidden, whole_down, preferred_element_type=jnp.float32)
    ffn_out = lax.psum_scatter(
        unit_terms.astype(jnp.bfloat16), "tp", scatter_dimension=1, tiled=True
    ).astype(jnp.float32)
    mixed_two = residual_scale * normed.astype(jnp.float32) + ffn_out
    totals_two = lax.psum((jnp.sum(mixed_two, 1), jnp.sum(mixed_two * mixed_two, 1)), "tp")
    return finish(mixed_two, totals_two, norm2_gain, norm2_bias).astype(jnp.bfloat16)


def solution(mesh):
    placed = (
        P("sp", "tp"),
        P("sp", "tp"),
        P("sp", "tp"),
        P("sp", None),
        P("sp", None),
        P("sp"),
        P(None, "tp"),
        P(None, "tp"),
        P("tp", None),
        P("tp"),
        P("tp"),
        P("sp", "tp"),
        P("sp", "tp"),
        P(None, "tp"),
        P(None, "tp"),
        P("tp", "sp"),
        P("tp"),
        P("tp"),
    )
    return jax.shard_map(
        local, mesh=mesh, in_specs=placed, out_specs=P("sp", "tp"), check_vma=False
    )
```

profile of v0, /device:TPU:0, one launch (start us, length us, event | category | flops | bytes accessed | tf_op | source)
XLA Modules:
  0.0 515.4 jit_solution(5412950258524241437)
XLA Ops:
  6.6 0.9 convert_element_type.119
  7.5 0.3 subtract_convert_fusion.1
  7.8 5.9 %collective-permute-start.6 = (bf16[384,64]{0,1:T(8,128)(2,1)S(1)}, bf16[384,64]{0,1:T(8,128)(2,1)S(1)}, u32[]{:S(2)}, u32[]{:S(2)}) collective-permute-start(bf16[384,64]{0,1:T(8,128)(2,1)S(1)} %pad_maximum_fusion.2), channel_id=1, source_target_pairs={{0,12},{4,16},{8,20},{12,24},{16,28},{1,13},{5,17},{9,21},{13,25},... | collective-permute-start | bytes 147464 | tf_op jit(solution)/shard_map/ppermute | solution.py:23
  13.7 3.5 collective-permute-start.7
  17.2 2.9 collective-permute-start.3
  20.1 1.9 collective-permute-start.4
  22.0 2.8 collective-permute-start.5
  24.8 1.2 copy.21
  26.0 0.1 subtract_convert_fusion
  26.2 2.6 collective-permute-start
  28.8 1.3 collective-permute-start.1
  30.1 3.1 collective-permute-start.2
  33.2 1.4 compare_and_fusion
  34.7 3.6 collective-permute-done
  38.3 2.2 collective-permute-start.8
  40.5 4.5 collective-permute-done.1
  45.1 0.0 copy-start.4
  45.1 1.9 convolution_convert_fusion
  47.0 8.0 %fusion.30 = f32[8,1536,384]{2,1,0:T(8,128)} fusion(bf16[1536,8,128]{0,2,1:T(8,128)(2,1)S(1)} %bitcast.40, bf16[384,1024]{1,0:T(8,128)(2,1)S(1)} %copy-done.4), kind=kOutput, calls=%fused_computation.46 | convolution fusion | flops 1207959552 | bytes 22806528 | tf_op jit(solution)/shard_map/qhd,khd->hqk/dot_general | solution.py:112
  55.0 12.0 %fusion.2 = f32[8,384,1536]{1,2,0:T(8,128)} fusion(f32[8,1536,384]{2,1,0:T(8,128)} %fusion.30, pred[384,1536]{0,1:T(8,128)(4,1)S(1)} %compare_and_fusion, bf16[384,8,32]{0,2,1:T(8,128)(2,1)S(1)} %get-tuple-element.20, bf16[384,8,32]{0,2,1:T(8,128)(2,1)S(1)} %get-tuple-element.19, bf16[384,32]{0,1:T(8,128)(2,1)S(1)} %get-tuple-element.22, ...), kind=kOutput, calls=%fused_computation.3 | convolution fusion | flops 619905024 | bytes 38928384 | tf_op jit(solution)/shard_map/qhr,kr->hqk/dot_general | solution.py:118
  67.1 15.3 %fusion.60 = f32[8,384]{1,0:T(8,128)S(1)} fusion(f32[8,384,1536]{1,2,0:T(8,128)} %fusion.2), kind=kOutput, calls=%fused_computation.114 | output fusion | flops 9438719 | bytes 18886656 | tf_op jit(solution)/shard_map/sub | solution.py:123
  82.4 3.5 convolution_convert_fusion.1
  86.0 17.5 %fusion.13 = bf16[8,128,384]{2,1,0:T(8,128)(2,1)S(1)} fusion(bf16[1536,8,128]{0,2,1:T(8,128)(2,1)} %bitcast.41, f32[8,384]{1,0:T(8,128)S(1)} %fusion.60, f32[8,384,1536]{1,2,0:T(8,128)} %fusion.2), kind=kOutput, calls=%fused_computation.24 | convolution fusion | flops 1222513152 | bytes 22818816 | tf_op jit(solution)/shard_map/hqk,khd->qhd/dot_general | solution.py:125
  103.5 0.0 copy-start.9
  103.5 0.0 copy-start.10
  103.5 0.0 copy-start.3
  103.5 5.2 %convolution_convert_fusion.5 = bf16[384,2048]{1,0:T(8,128)(2,1)} fusion(bf16[384,1024]{0,1:T(8,128)(2,1)S(1)} %bitcast.42, bf16[1024,2048]{1,0:T(8,128)(2,1)} %param.26), kind=kOutput, calls=%fused_computation.13 | convolution fusion | flops 1611399168 | bytes 6553600 | tf_op jit(solution)/shard_map/dot_general | solution.py:132
  108.7 0.0 reduce-scatter.3.cloned.1.call-update
  108.8 0.0 all-gather.5.cloned.1.call-start
  108.9 0.0 copy-start.7
  108.9 0.0 copy-start.8
  108.9 44.3 %reduce-scatter.3.cloned.1.call-done = bf16[384,512]{1,0:T(8,128)(2,1)} async-done(((bf16[384,2048]{1,0:T(8,128)(2,1)}), bf16[384,512]{1,0:T(8,128)(2,1)}) %reduce-scatter.3.cloned.1.call-update) | async-done | bytes 393232 | tf_op jit(solution)/shard_map/reduce_scatter | solution.py:133
  153.2 1.3 fusion.33
  154.4 5.8 %all-reduce.1 = (f32[384]{0:T(512)S(1)}, f32[384]{0:T(512)S(1)}) all-reduce(f32[384]{0:T(512)S(1)} %get-tuple-element.8, f32[384]{0:T(512)S(1)} %get-tuple-element.7), channel_id=1, replica_groups=mesh['sp'=8,'tp'=4] {'tp'}, use_global_device_ids=true, to_apply=%region_6.7 | all-reduce | flops 768 | bytes 6144 | tf_op jit(solution)/shard_map/psum | solution.py:137
  160.2 2.0 add_convert_fusion.1
  162.2 0.0 all-gather.5.cloned.1.call-update
  162.2 0.0 all-gather.9.cloned.1.call-start
  162.3 0.7 all-gather.9.cloned.1.call-update
  163.0 0.0 all-gather.7.cloned.1.call-start
  163.0 0.5 all-gather.7.cloned.1.call-update
  163.5 0.0 all-gather.11.cloned.1.call-start
  163.6 0.5 all-gather.11.cloned.1.call-update
  164.1 0.0 reduce-scatter.5.cloned.1.call-start
  164.2 0.1 slice.64
  164.2 3.5 collective-permute-start.10
  167.8 0.1 convert_reduce_fusion.2
  167.9 1.1 collective-permute-done.10
  169.0 0.1 pad_add_fusion.1
  169.1 13.5 %all-gather.5.cloned.1.call-done = bf16[384,2048]{1,0:T(8,128)(2,1)} async-done(((bf16[384,512]{1,0:T(8,128)(2,1)}), bf16[384,2048]{1,0:T(8,128)(2,1)}) %all-gather.5.cloned.1.call-update) | async-done | bytes 1572880 | tf_op jit(solution)/shard_map/all_gather | solution.py:139
  182.6 94.6 %all-gather.9.cloned.1.call-done = bf16[2048,1408]{1,0:T(8,128)(2,1)} async-done(((bf16[256,1408]{1,0:T(8,128)(2,1)}), bf16[2048,1408]{1,0:T(8,128)(2,1)}) %all-gather.9.cloned.1.call-update) | async-done | bytes 5767184 | tf_op jit(solution)/shard_map/all_gather | solution.py:78
  277.2 5.7 %convolution_convert_fusion.3 = bf16[384,1408]{1,0:T(8,128)(2,1)S(1)} fusion(bf16[384,2048]{1,0:T(8,128)(2,1)} %all-gather.5.cloned.1.call-done, bf16[2048,1408]{1,0:T(8,128)(2,1)} %all-gather.9.cloned.1.call-done), kind=kOutput, calls=%fused_computation.11 | convolution fusion | flops 2215133184 | bytes 8421376 | tf_op jit(solution)/shard_map/dot_general | solution.py:140
  283.0 1.0 copy-done.13
  284.0 2.7 collective-permute-start.11
  286.7 83.1 %all-gather.7.cloned.1.call-done = bf16[2048,1408]{1,0:T(8,128)(2,1)} async-done(((bf16[256,1408]{1,0:T(8,128)(2,1)}), bf16[2048,1408]{1,0:T(8,128)(2,1)}) %all-gather.7.cloned.1.call-update) | async-done | bytes 5767184 | tf_op jit(solution)/shard_map/all_gather | solution.py:79
  369.8 5.7 %convolution_convert_fusion.4 = bf16[384,1408]{1,0:T(8,128)(2,1)S(1)} fusion(bf16[384,2048]{1,0:T(8,128)(2,1)} %all-gather.5.cloned.1.call-done, bf16[2048,1408]{1,0:T(8,128)(2,1)} %all-gather.7.cloned.1.call-done), kind=kOutput, calls=%fused_computation.12 | convolution fusion | flops 2215133184 | bytes 8421376 | tf_op jit(solution)/shard_map/dot_general | solution.py:141
  375.5 2.5 collective-permute-start.9
  378.0 0.1 fusion.49
  378.1 84.9 %all-gather.11.cloned.1.call-done = bf16[1408,2048]{1,0:T(8,128)(2,1)} async-done(((bf16[1408,256]{1,0:T(8,128)(2,1)}), bf16[1408,2048]{1,0:T(8,128)(2,1)}) %all-gather.11.cloned.1.call-update) | async-done | bytes 5767184 | tf_op jit(solution)/shard_map/all_gather | solution.py:80
  463.1 10.1 %convolution_convert_fusion.2 = bf16[384,2048]{1,0:T(8,128)(2,1)} fusion(bf16[1408,2048]{1,0:T(8,128)(2,1)} %all-gather.11.cloned.1.call-done, bf16[384,1408]{1,0:T(8,128)(2,1)} %copy-done.13, bf16[384,1408]{1,0:T(8,128)(2,1)} %copy-done.14, bf16[2,1408]{1,0:T(2,128)(2,1)S(1)} %collective-permute-done.11, bf16[2,1408]{1,0:T(2,128)(2,1)S(1)} %collective-permute-done.9, ...), kind=kOutput, calls=%fused_computation.10 | convolution fusion | flops 2239168512 | bytes 9552384 | tf_op jit(solution)/shard_map/dot_general | solution.py:176
  473.2 0.0 reduce-scatter.5.cloned.1.call-update
  473.3 26.3 %reduce-scatter.5.cloned.1.call-done = bf16[384,512]{1,0:T(8,128)(2,1)} async-done(((bf16[384,2048]{1,0:T(8,128)(2,1)}), bf16[384,512]{1,0:T(8,128)(2,1)}) %reduce-scatter.5.cloned.1.call-update) | async-done | bytes 393232 | tf_op jit(solution)/shard_map/reduce_scatter | solution.py:177
  499.6 1.3 fusion.34
  500.8 5.8 %all-reduce = (f32[384]{0:T(512)S(1)}, f32[384]{0:T(512)S(1)}) all-reduce(f32[384]{0:T(512)S(1)} %get-tuple-element.6, f32[384]{0:T(512)S(1)} %get-tuple-element.5), channel_id=1, replica_groups=mesh['sp'=8,'tp'=4] {'tp'}, use_global_device_ids=true, to_apply=%region_11.12 | all-reduce | flops 768 | bytes 6144 | tf_op jit(solution)/shard_map/psum | solution.py:181
  506.6 2.0 add_convert_fusion
  (55 shorter events, 0.3 us)
Async XLA Ops:
  6.5 38.6 %copy-start = (bf16[512,1024]{1,0:T(8,128)(2,1)S(1)}, bf16[512,1024]{1,0:T(8,128)(2,1)}, u32[]{:S(2)}) copy-start(bf16[512,1024]{1,0:T(8,128)(2,1)} %param.24) | copy-start | bytes 3145732
  6.5 26.7 %copy-start.6 = (s32[384]{0:T(512)S(1)}, s32[384]{0:T(512)}, u32[]{:S(2)}) copy-start(s32[384]{0:T(512)} %param.23) | copy-start | bytes 4612
  6.5 19.6 %copy-start.5 = (bf16[384,512]{1,0:T(8,128)(2,1)S(1)}, bf16[384,512]{1,0:T(8,128)(2,1)}, u32[]{:S(2)}) copy-start(bf16[384,512]{1,0:T(8,128)(2,1)} %param.21) | copy-start | bytes 1179652
  6.5 146.6 %reduce-scatter.3.cloned.1.call-start = ((), (), s32[]{:S(2)}) async-start(), calls=%async_computation.2 | async-start | bytes 1966080 | tf_op jit(solution)/shard_map/reduce_scatter | solution.py:133
  7.8 47.2 %collective-permute-start.6 = (bf16[384,64]{0,1:T(8,128)(2,1)S(1)}, bf16[384,64]{0,1:T(8,128)(2,1)S(1)}, u32[]{:S(2)}, u32[]{:S(2)}) collective-permute-start(bf16[384,64]{0,1:T(8,128)(2,1)S(1)} %pad_maximum_fusion.2), channel_id=1, source_target_pairs={{0,12},{4,16},{8,20},{12,24},{16,28},{1,13},{5,17},{9,21},{13,25},... | collective-permute-start | bytes 147464 | tf_op jit(solution)/shard_map/ppermute | solution.py:23
  13.7 41.3 %collective-permute-start.7 = (bf16[384,64]{0,1:T(8,128)(2,1)S(1)}, bf16[384,64]{0,1:T(8,128)(2,1)S(1)}, u32[]{:S(2)}, u32[]{:S(2)}) collective-permute-start(bf16[384,64]{0,1:T(8,128)(2,1)S(1)} %pad_maximum_fusion.2), channel_id=1, source_target_pairs={{0,8},{4,12},{8,16},{12,20},{16,24},{20,28},{1,9},{5,13},{9,17},{1... | collective-permute-start | bytes 147464 | tf_op jit(solution)/shard_map/ppermute | solution.py:23
  17.2 8.9 %collective-permute-start.3 = (s32[384]{0:T(512)}, s32[384]{0:T(512)S(1)}, u32[]{:S(2)}, u32[]{:S(2)}) collective-permute-start(s32[384]{0:T(512)} %param.23), channel_id=1, source_target_pairs={{0,12},{4,16},{8,20},{12,24},{16,28},{1,13},{5,17},{9,21},{13,25},... | collective-permute-start | bytes 4616 | tf_op jit(solution)/shard_map/ppermute | solution.py:23
  20.1 8.6 %collective-permute-start.4 = (s32[384]{0:T(512)}, s32[384]{0:T(512)S(1)}, u32[]{:S(2)}, u32[]{:S(2)}) collective-permute-start(s32[384]{0:T(512)} %param.23), channel_id=1, source_target_pairs={{0,8},{4,12},{8,16},{12,20},{16,24},{20,28},{1,9},{5,13},{9,17},{1... | collective-permute-start | bytes 4616 | tf_op jit(solution)/shard_map/ppermute | solution.py:23
  22.0 8.1 %collective-permute-start.5 = (s32[384]{0:T(512)}, s32[384]{0:T(512)S(1)}, u32[]{:S(2)}, u32[]{:S(2)}) collective-permute-start(s32[384]{0:T(512)} %param.23), channel_id=1, source_target_pairs={{0,4},{4,8},{8,12},{12,16},{16,20},{20,24},{24,28},{1,5},{5,9},{9,... | collective-permute-start | bytes 4616 | tf_op jit(solution)/shard_map/ppermute | solution.py:23
  26.2 12.1 %collective-permute-start = (bf16[384,512]{1,0:T(8,128)(2,1)S(1)}, bf16[384,512]{1,0:T(8,128)(2,1)S(1)}, u32[]{:S(2)}, u32[]{:S(2)}) collective-permute-start(bf16[384,512]{1,0:T(8,128)(2,1)S(1)} %copy-done.5), channel_id=1, source_target_pairs={{0,12},{4,16},{8,20},{12,24},{16,28},{1,13},{5,17},{9,21},{13,25},... | collective-permute-start | bytes 1179656 | tf_op jit(solution)/shard_map/ppermute | solution.py:23
  28.8 16.2 %collective-permute-start.1 = (bf16[384,512]{1,0:T(8,128)(2,1)S(1)}, bf16[384,512]{1,0:T(8,128)(2,1)S(1)}, u32[]{:S(2)}, u32[]{:S(2)}) collective-permute-start(bf16[384,512]{1,0:T(8,128)(2,1)S(1)} %copy-done.5), channel_id=1, source_target_pairs={{0,8},{4,12},{8,16},{12,20},{16,24},{20,28},{1,9},{5,13},{9,17},{1... | collective-permute-start | bytes 1179656 | tf_op jit(solution)/shard_map/ppermute | solution.py:23
  30.1 14.9 %collective-permute-start.2 = (bf16[384,512]{1,0:T(8,128)(2,1)S(1)}, bf16[384,512]{1,0:T(8,128)(2,1)S(1)}, u32[]{:S(2)}, u32[]{:S(2)}) collective-permute-start(bf16[384,512]{1,0:T(8,128)(2,1)S(1)} %copy-done.5), channel_id=1, source_target_pairs={{0,4},{4,8},{8,12},{12,16},{16,20},{20,24},{24,28},{1,5},{5,9},{9,... | collective-permute-start | bytes 1179656 | tf_op jit(solution)/shard_map/ppermute | solution.py:23
  38.3 16.8 %collective-permute-start.8 = (bf16[384,64]{0,1:T(8,128)(2,1)S(1)}, bf16[384,64]{0,1:T(8,128)(2,1)S(1)}, u32[]{:S(2)}, u32[]{:S(2)}) collective-permute-start(bf16[384,64]{0,1:T(8,128)(2,1)S(1)} %pad_maximum_fusion.2), channel_id=1, source_target_pairs={{0,4},{4,8},{8,12},{12,16},{16,20},{20,24},{24,28},{1,5},{5,9},{9,... | collective-permute-start | bytes 147464 | tf_op jit(solution)/shard_map/ppermute | solution.py:23
  45.1 1.9 copy-start.4
  67.1 15.4 %copy-start.15 = (bf16[512,1024]{1,0:T(8,128)(2,1)S(1)}, bf16[512,1024]{1,0:T(8,128)(2,1)}, u32[]{:S(2)}) copy-start(bf16[512,1024]{1,0:T(8,128)(2,1)} %param.25) | copy-start | bytes 3145732
  103.5 5.3 %copy-start.9 = (bf16[512]{0:T(512)(128)(2,1)S(1)}, bf16[512]{0:T(512)(128)(2,1)}, u32[]{:S(2)}) copy-start(bf16[512]{0:T(512)(128)(2,1)} %param.27) | copy-start | bytes 3076
  103.5 5.3 %copy-start.10 = (bf16[512]{0:T(512)(128)(2,1)S(1)}, bf16[512]{0:T(512)(128)(2,1)}, u32[]{:S(2)}) copy-start(bf16[512]{0:T(512)(128)(2,1)} %param.28) | copy-start | bytes 3076
  103.5 49.7 %copy-start.3 = (bf16[384,512]{1,0:T(8,128)(2,1)S(1)}, bf16[384,512]{1,0:T(8,128)(2,1)}, u32[]{:S(2)}) copy-start(bf16[384,512]{1,0:T(8,128)(2,1)} %param.18) | copy-start | bytes 1179652
  108.8 73.9 %all-gather.5.cloned.1.call-start = ((), (), s32[]{:S(2)}) async-start(), calls=%async_computation.3 | async-start | bytes 1966080 | tf_op jit(solution)/shard_map/all_gather | solution.py:139
  108.9 58.9 %copy-start.7 = (bf16[3,1408]{1,0:T(4,128)(2,1)S(1)}, bf16[3,1408]{1,0:T(4,128)(2,1)}, u32[]{:S(2)}) copy-start(bf16[3,1408]{1,0:T(4,128)(2,1)} %param.31) | copy-start | bytes 25348
  108.9 58.9 %copy-start.8 = (bf16[3,1408]{1,0:T(4,128)(2,1)S(1)}, bf16[3,1408]{1,0:T(4,128)(2,1)}, u32[]{:S(2)}) copy-start(bf16[3,1408]{1,0:T(4,128)(2,1)} %param.32) | copy-start | bytes 25348
  162.2 115.0 %all-gather.9.cloned.1.call-start = ((), (), s32[]{:S(2)}) async-start(), calls=%async_computation.5 | async-start | bytes 6488064 | tf_op jit(solution)/shard_map/all_gather | solution.py:78
  163.0 206.8 %all-gather.7.cloned.1.call-start = ((), (), s32[]{:S(2)}) async-start(), calls=%async_computation.4 | async-start | bytes 6488064 | tf_op jit(solution)/shard_map/all_gather | solution.py:79
  163.5 299.5 %all-gather.11.cloned.1.call-start = ((), (), s32[]{:S(2)}) async-start(), calls=%async_computation.6 | async-start | bytes 6488064 | tf_op jit(solution)/shard_map/all_gather | solution.py:80
  164.1 335.5 %reduce-scatter.5.cloned.1.call-start = ((), (), s32[]{:S(2)}) async-start(), calls=%async_computation.7 | async-start | bytes 1966080 | tf_op jit(solution)/shard_map/reduce_scatter | solution.py:177
  164.2 4.8 collective-permute-start.10
  282.9 1.0 copy-start.13
  284.0 179.1 %collective-permute-start.11 = (bf16[2,1408]{1,0:T(2,128)(2,1)S(1)}, bf16[2,1408]{1,0:T(2,128)(2,1)S(1)}, u32[]{:S(2)}, u32[]{:S(2)}) collective-permute-start(bf16[2,1408]{1,0:T(2,128)(2,1)S(1)} %slice.83), channel_id=1, source_target_pairs={{0,4},{4,8},{8,12},{12,16},{16,20},{20,24},{24,28},{1,5},{5,9},{9,... | collective-permute-start | bytes 16904 | tf_op jit(solution)/shard_map/ppermute | solution.py:23
  375.5 2.5 copy-start.14
  375.5 87.5 %collective-permute-start.9 = (bf16[2,1408]{1,0:T(2,128)(2,1)S(1)}, bf16[2,1408]{1,0:T(2,128)(2,1)S(1)}, u32[]{:S(2)}, u32[]{:S(2)}) collective-permute-start(bf16[2,1408]{1,0:T(2,128)(2,1)S(1)} %slice.80), channel_id=1, source_target_pairs={{0,4},{4,8},{8,12},{12,16},{16,20},{20,24},{24,28},{1,5},{5,9},{9,... | collective-permute-start | bytes 16904 | tf_op jit(solution)/shard_map/ppermute | solution.py:23
  463.0 10.2 %copy-start.11 = (bf16[512]{0:T(512)(128)(2,1)S(1)}, bf16[512]{0:T(512)(128)(2,1)}, u32[]{:S(2)}) copy-start(bf16[512]{0:T(512)(128)(2,1)} %param.34) | copy-start | bytes 3076
  463.0 10.2 %copy-start.12 = (bf16[512]{0:T(512)(128)(2,1)S(1)}, bf16[512]{0:T(512)(128)(2,1)}, u32[]{:S(2)}) copy-start(bf16[512]{0:T(512)(128)(2,1)} %param.35) | copy-start | bytes 3076
  463.0 36.5 %copy-start.2 = (bf16[384,512]{1,0:T(8,128)(2,1)S(1)}, bf16[384,512]{1,0:T(8,128)(2,1)}, u32[]{:S(2)}) copy-start(bf16[384,512]{1,0:T(8,128)(2,1)} %add_convert_fusion.1) | copy-start | bytes 1179652
  463.1 45.5 %copy-start.1 = (bf16[512,1024]{1,0:T(8,128)(2,1)S(1)}, bf16[512,1024]{1,0:T(8,128)(2,1)}, u32[]{:S(2)}) copy-start(bf16[512,1024]{1,0:T(8,128)(2,1)} %param.24) | copy-start | bytes 3145732
Sparse Core Ops, SparseCore 0:
  108.9 44.2 reduce-scatter.2
  162.3 20.2 all-gather.4
  184.8 92.3 all-gather.8
  279.3 90.4 all-gather.6
  371.7 91.3 all-gather.10
  473.3 26.1 reduce-scatter.4
where the time goes:
time: 516 us; the launch traced here: 515 us
  waiting for transfers between devices  358 us (69%)
  matrix products  69.7 us (14%)
  starting transfers between devices  35 us (7%)
  other arithmetic  24.9 us (5%)
  between operations  14 us (3%)
  blocking collectives  11.5 us (2%)
    all_gather x1, waiting for transfers between devices, local(): lax.all_gather(ffn_gate, 'sp', axis=0, tiled=True)  94.6 us
    all_gather x1, waiting for transfers between devices, local(): lax.all_gather(ffn_down, 'sp', axis=1, tiled=True)  84.9 us
    all_gather x1, waiting for transfers between devices, local(): lax.all_gather(ffn_value, 'sp', axis=0, tiled=True)  83.1 us
    reduce_scatter x1, waiting for transfers between devices, local(): lax.psum_scatter(head_terms.astype(jnp.bfloat16), 'tp', scatter_dimension...  44.3 us
    ppermute x12, starting transfers between devices, passed_along(): return lax.ppermute(value, axis, pairs)  34.8 us
    reduce_scatter x1, waiting for transfers between devices, local(): lax.psum_scatter(unit_terms.astype(jnp.bfloat16), 'tp', scatter_dimension...  26.3 us
    dot_general x1, matrix products, local(): jnp.einsum('hqk,khd->qhd', weights, values.reshape(window, head_count, VD...  17.5 us
    sub x1, other arithmetic, local(): weights = jnp.exp(scores - row_max)  15.3 us
  transfers between devices with their start and end apart: 18, of which 9 were waited for; matrix products, arithmetic and copies ran while one was open for 5% of the time, Pallas kernels for 0%

commit v1 on v0

--- a/solution.py
+++ b/solution.py
@@ -40,6 +40,14 @@
         ],
         axis=-1,
     )
+
+
+def scatter_sum(terms, axis):
+    count = lax.axis_size(axis)
+    width = terms.shape[1] // count
+    parts = jnp.stack([terms[:, i * width : (i + 1) * width] for i in range(count)])
+    got = lax.all_to_all(parts.astype(jnp.bfloat16), axis, 0, 0)
+    return jnp.sum(got.astype(jnp.float32), 0)
 
 
 def finish(mixed, totals, gain_row, bias_row):
@@ -130,13 +138,18 @@
     )
     attended = attended.astype(jnp.bfloat16).reshape(row_count, head_count * VDIM)
     head_terms = jnp.dot(attended, out_proj, preferred_element_type=jnp.float32)
-    projected = lax.psum_scatter(
-        head_terms.astype(jnp.bfloat16), "tp", scatter_dimension=1, tiled=True
-    ).astype(jnp.float32)
+    projected = scatter_sum(head_terms, "tp")
     mixed_one = residual_scale * residual.astype(jnp.float32) + projected
     totals_one = lax.psum((jnp.sum(mixed_one, 1), jnp.sum(mixed_one * mixed_one, 1)), "tp")
     normed = finish(mixed_one, totals_one, norm1_gain, norm1_bias).astype(jnp.bfloat16)
-    full_rows = lax.all_gather(normed, "tp", axis=1, tiled=True)
+    half = row_count // 2
+    full_rows = jnp.concatenate(
+        [
+            lax.all_gather(normed[:half], "tp", axis=1, tiled=True),
+            lax.all_gather(normed[half:], "tp", axis=1, tiled=True),
+        ],
+        0,
+    )
     gate_sum = jnp.dot(full_rows, whole_gate, preferred_element_type=jnp.float32)
     value_sum = jnp.dot(full_rows, whole_value, preferred_element_type=jnp.float32)
     gate_pre = gate_sum.astype(jnp.bfloat16)
@@ -174,9 +187,7 @@
         )
     hidden = (value_mix * jax.nn.gelu(gate_mix)).astype(jnp.bfloat16)
     unit_terms = jnp.dot(hidden, whole_down, preferred_element_type=jnp.float32)
-    ffn_out = lax.psum_scatter(
-        unit_terms.astype(jnp.bfloat16), "tp", scatter_dimension=1, tiled=True
-    ).astype(jnp.float32)
+    ffn_out = scatter_sum(unit_terms, "tp")
     mixed_two = residual_scale * normed.astype(jnp.float32) + ffn_out
     totals_two = lax.psum((jnp.sum(mixed_two, 1), jnp.sum(mixed_two * mixed_two, 1)), "tp")
     return finish(mixed_two, totals_two, norm2_gain, norm2_bias).astype(jnp.bfloat16)

time: 516 us -> 368 us (0.71)
  waiting for transfers between devices: 358 us -> 167 us
  starting transfers between devices: 35 us -> 62.4 us
  blocking collectives: 11.5 us -> 28.9 us
    all_gather x1, waiting for transfers between devices: 94.6 us -> 0.02 us  [local(): lax.all_gather(ffn_gate, 'sp', axis=0, tiled=True)]
    reduce_scatter x2 -> x0, waiting for transfers between devices: 70.6 us -> none  [the longest x1 44.3 us: local(): lax.psum_scatter(head_terms.astype(jnp.bfloat16), 'tp', scatter_dimension...]
    all_gather x1, waiting for transfers between devices: 83.1 us -> 30.3 us  [local(): lax.all_gather(ffn_value, 'sp', axis=0, tiled=True)]
    all_to_all x0 -> x2, waiting for transfers between devices: none -> 26.1 us  [scatter_sum(): got = lax.all_to_all(parts.astype(jnp.bfloat16), axis, 0, 0)]
    ppermute x12, starting transfers between devices: 34.8 us -> 55 us  [passed_along(): return lax.ppermute(value, axis, pairs)]
    all_gather x0 -> x2, blocking collectives: none -> 17.1 us  [the longest x1 8.71 us: local(): lax.all_gather(normed[half:], 'tp', axis=1, tiled=True)]
    ppermute x12, waiting for transfers between devices: 9.25 us -> 23.9 us  [passed_along(): return lax.ppermute(value, axis, pairs)]
    all_gather x1 -> x0, waiting for transfers between devices: 13.5 us -> none  [local(): full_rows = lax.all_gather(normed, 'tp', axis=1, tiled=True)]
  transfers between devices with their start and end apart: 18 -> 17, of which waited for: 9 -> 7; matrix products, arithmetic and copies ran while one was open for 5% -> 22% of each run, Pallas kernels for 0% -> 0%
where the time goes in v1:
time: 368 us; the launch traced here: 367 us
  waiting for transfers between devices  167 us (45%)
  matrix products  67.2 us (18%)
  starting transfers between devices  62.4 us (17%)
  blocking collectives  28.9 us (8%)
  other arithmetic  25.2 us (7%)
  between operations  13.7 us (4%)
    all_gather x1, waiting for transfers between devices, local(): lax.all_gather(ffn_down, 'sp', axis=1, tiled=True)  85.7 us
    ppermute x12, starting transfers between devices, passed_along(): return lax.ppermute(value, axis, pairs)  55 us
    all_gather x1, waiting for transfers between devices, local(): lax.all_gather(ffn_value, 'sp', axis=0, tiled=True)  30.3 us
    all_to_all x2, waiting for transfers between devices, scatter_sum(): got = lax.all_to_all(parts.astype(jnp.bfloat16), axis, 0, 0)  26.1 us
    ppermute x12, waiting for transfers between devices, passed_along(): return lax.ppermute(value, axis, pairs)  23.9 us
    dot_general x1, matrix products, local(): jnp.einsum('hqk,khd->qhd', weights, values.reshape(window, head_count, VD...  17.6 us
    sub x1, other arithmetic, local(): weights = jnp.exp(scores - row_max)  15.4 us
    dot_general x1, matrix products, local(): jnp.einsum('qhr,kr->hqk', turned_query, win_key, preferred_element_type=j...  12.1 us
  transfers between devices with their start and end apart: 17, of which 7 were waited for; matrix products, arithmetic and copies ran while one was open for 22% of the time, Pallas kernels for 0%

profile of v1, /device:TPU:0, one launch (start us, length us, event | category | flops | bytes accessed | tf_op | source)
XLA Modules:
  0.0 366.7 jit_solution(3545293043475565079)
XLA Ops:
  6.5 0.7 all-gather.6.cloned.1.call-update
  7.3 0.0 copy-start.7
  7.3 0.0 all-gather.4.cloned.1.call-start
  7.3 0.7 all-gather.4.cloned.1.call-update
  8.0 0.0 all-gather.8.cloned.1.call-start
  8.1 0.8 convert_element_type.115
  8.9 0.3 subtract_convert_fusion.1
  9.2 5.9 %collective-permute-start.6 = (bf16[384,64]{0,1:T(8,128)(2,1)S(1)}, bf16[384,64]{0,1:T(8,128)(2,1)S(1)}, u32[]{:S(2)}, u32[]{:S(2)}) collective-permute-start(bf16[384,64]{0,1:T(8,128)(2,1)S(1)} %pad_maximum_fusion.4), channel_id=1, source_target_pairs={{0,12},{4,16},{8,20},{12,24},{16,28},{1,13},{5,17},{9,21},{13,25},... | collective-permute-start | bytes 147464 | tf_op jit(solution)/shard_map/ppermute | solution.py:23
  15.1 3.5 collective-permute-start.7
  18.6 2.9 collective-permute-start.3
  21.5 1.9 collective-permute-start.4
  23.4 2.8 collective-permute-start.5
  26.2 0.0 all-gather.8.cloned.1.call-update
  26.3 0.2 copy.21
  26.4 0.1 subtract_convert_fusion
  26.6 2.6 collective-permute-start
  29.2 1.3 collective-permute-start.1
  30.5 3.4 collective-permute-start.2
  33.9 1.4 compare_and_fusion
  35.3 11.7 %collective-permute-done = bf16[384,512]{1,0:T(8,128)(2,1)S(1)} collective-permute-done((bf16[384,512]{1,0:T(8,128)(2,1)S(1)}, bf16[384,512]{1,0:T(8,128)(2,1)S(1)}, u32[]{:S(2)}, u32[]{:S(2)}) %collective-permute-start) | collective-permute-done | bytes 393248 | tf_op jit(solution)/shard_map/ppermute | solution.py:23
  47.1 3.3 collective-permute-start.8
  50.4 11.0 %collective-permute-done.1 = bf16[384,512]{1,0:T(8,128)(2,1)S(1)} collective-permute-done((bf16[384,512]{1,0:T(8,128)(2,1)S(1)}, bf16[384,512]{1,0:T(8,128)(2,1)S(1)}, u32[]{:S(2)}, u32[]{:S(2)}) %collective-permute-start.1) | collective-permute-done | bytes 393248 | tf_op jit(solution)/shard_map/ppermute | solution.py:23
  61.6 1.9 convolution_convert_fusion
  63.5 8.3 %fusion.30 = f32[8,1536,384]{2,1,0:T(8,128)} fusion(bf16[1536,8,128]{0,2,1:T(8,128)(2,1)S(1)} %bitcast.56, bf16[384,1024]{1,0:T(8,128)(2,1)S(1)} %copy-done.4), kind=kOutput, calls=%fused_computation.50 | convolution fusion | flops 1207959552 | bytes 22806528 | tf_op jit(solution)/shard_map/qhd,khd->hqk/dot_general | solution.py:120
  71.8 3.5 convolution_convert_fusion.1
  75.3 12.1 %fusion.2 = f32[8,384,1536]{1,2,0:T(8,128)} fusion(f32[8,1536,384]{2,1,0:T(8,128)} %fusion.30, pred[384,1536]{0,1:T(8,128)(4,1)S(1)} %compare_and_fusion, bf16[384,8,32]{0,2,1:T(8,128)(2,1)S(1)} %get-tuple-element.28, bf16[384,8,32]{0,2,1:T(8,128)(2,1)S(1)} %get-tuple-element.27, bf16[384,32]{0,1:T(8,128)(2,1)S(1)} %get-tuple-element.32, ...), kind=kOutput, calls=%fused_computation.3 | convolution fusion | flops 619905024 | bytes 38928384 | tf_op jit(solution)/shard_map/qhr,kr->hqk/dot_general | solution.py:126
  87.4 15.4 %fusion.61 = f32[8,384]{1,0:T(8,128)S(1)} fusion(f32[8,384,1536]{1,2,0:T(8,128)} %fusion.2), kind=kOutput, calls=%fused_computation.129 | output fusion | flops 9438719 | bytes 18886656 | tf_op jit(solution)/shard_map/sub | solution.py:131
  102.8 17.6 %fusion.13 = bf16[8,128,384]{2,1,0:T(8,128)(2,1)S(1)} fusion(bf16[1536,8,128]{0,2,1:T(8,128)(2,1)} %bitcast.57, f32[8,384]{1,0:T(8,128)S(1)} %fusion.61, f32[8,384,1536]{1,2,0:T(8,128)} %fusion.2), kind=kOutput, calls=%fused_computation.28 | convolution fusion | flops 1222513152 | bytes 22818816 | tf_op jit(solution)/shard_map/hqk,khd->qhd/dot_general | solution.py:133
  120.4 4.0 %convolution_convert_fusion.5 = bf16[384,2048]{1,0:T(8,128)(2,1)S(1)} fusion(bf16[384,1024]{0,1:T(8,128)(2,1)S(1)} %bitcast.58, bf16[1024,2048]{1,0:T(8,128)(2,1)} %param.26), kind=kOutput, calls=%fused_computation.15 | convolution fusion | flops 1611399168 | bytes 6553600 | tf_op jit(solution)/shard_map/dot_general | solution.py:140
  124.4 0.1 slice_bitcast_fusion.7
  124.6 1.4 pad_maximum_fusion
  125.9 3.7 %all-to-all-start = ((bf16[4,384,512]{2,1,0:T(8,128)(2,1)}), bf16[4,384,512]{2,1,0:T(8,128)(2,1)S(1)}, u32[]{:S(2)}, u32[]{:S(2)}) async-start(bf16[4,384,512]{2,1,0:T(8,128)(2,1)} %pad_maximum_fusion), calls=%async_computation | async-start | bytes 3145728 | tf_op jit(solution)/shard_map/all_to_all | solution.py:49
  129.7 0.1 slice.108
  129.7 12.4 %collective-permute-start.10 = (s32[2]{0:T(128)S(1)}, s32[2]{0:T(128)S(1)}, u32[]{:S(2)}, u32[]{:S(2)}) collective-permute-start(s32[2]{0:T(128)S(1)} %slice.108), channel_id=1, source_target_pairs={{0,4},{4,8},{8,12},{12,16},{16,20},{20,24},{24,28},{1,5},{5,9},{9,... | collective-permute-start | bytes 32 | tf_op jit(solution)/shard_map/ppermute | solution.py:23
  142.3 0.1 convert_reduce_fusion.4
  142.4 1.1 collective-permute-done.10
  143.5 0.1 pad_add_fusion.1
  143.5 6.1 %all-to-all-done = bf16[4,384,512]{2,1,0:T(8,128)(2,1)S(1)} async-done(((bf16[4,384,512]{2,1,0:T(8,128)(2,1)}), bf16[4,384,512]{2,1,0:T(8,128)(2,1)S(1)}, u32[]{:S(2)}, u32[]{:S(2)}) %all-to-all-start) | async-done | bytes 1572896 | tf_op jit(solution)/shard_map/all_to_all | solution.py:49
  149.7 0.2 convert_reduce_fusion.1
  149.9 0.2 fusion.36
  150.2 6.1 %all-reduce.1 = (f32[384]{0:T(512)S(1)}, f32[384]{0:T(512)S(1)}) all-reduce(f32[384]{0:T(512)S(1)} %get-tuple-element.8, f32[384]{0:T(512)S(1)} %get-tuple-element.7), channel_id=1, replica_groups=mesh['sp'=8,'tp'=4] {'tp'}, use_global_device_ids=true, to_apply=%region_6.7 | all-reduce | flops 768 | bytes 6144 | tf_op jit(solution)/shard_map/psum | solution.py:143
  156.2 0.2 add_convert_fusion.1
  156.5 8.4 %all_gather.15 = bf16[192,2048]{1,0:T(8,128)(2,1)S(1)} all-gather(bf16[192,512]{1,0:T(8,128)(2,1)S(1)} %get-tuple-element.30), channel_id=1, replica_groups=mesh['sp'=8,'tp'=4] {'tp'}, dimensions={1}, use_global_device_ids=true | all-gather | bytes 983040 | tf_op jit(solution)/shard_map/all_gather | solution.py:148
  164.9 0.1 constant_dynamic-update-slice_fusion.5
  165.0 8.7 %all_gather.16 = bf16[192,2048]{1,0:T(8,128)(2,1)S(1)} all-gather(bf16[192,512]{1,0:T(8,128)(2,1)S(1)} %get-tuple-element.29), channel_id=1, replica_groups=mesh['sp'=8,'tp'=4] {'tp'}, dimensions={1}, use_global_device_ids=true | all-gather | bytes 983040 | tf_op jit(solution)/shard_map/all_gather | solution.py:149
  173.7 0.1 constant_dynamic-update-slice_fusion.4
  173.7 0.0 all-gather.6.cloned.1.call-done
  173.7 5.2 %convolution_convert_fusion.3 = bf16[384,1408]{1,0:T(8,128)(2,1)S(1)} fusion(bf16[384,2048]{1,0:T(8,128)(2,1)S(1)} %constant_dynamic-update-slice_fusion.4, bf16[2048,1408]{1,0:T(8,128)(2,1)} %all-gather.6.cloned.1.call-done), kind=kOutput, calls=%fused_computation.13 | convolution fusion | flops 2215133184 | bytes 8421376 | tf_op jit(solution)/shard_map/dot_general | solution.py:153
  179.0 1.0 copy-done.14
  180.0 12.5 %collective-permute-start.11 = (bf16[2,1408]{1,0:T(2,128)(2,1)S(1)}, bf16[2,1408]{1,0:T(2,128)(2,1)S(1)}, u32[]{:S(2)}, u32[]{:S(2)}) collective-permute-start(bf16[2,1408]{1,0:T(2,128)(2,1)S(1)} %slice.137), channel_id=1, source_target_pairs={{0,4},{4,8},{8,12},{12,16},{16,20},{20,24},{24,28},{1,5},{5,9},{9,... | collective-permute-start | bytes 16904 | tf_op jit(solution)/shard_map/ppermute | solution.py:23
  192.5 30.3 %all-gather.4.cloned.1.call-done = bf16[2048,1408]{1,0:T(8,128)(2,1)} async-done(((bf16[256,1408]{1,0:T(8,128)(2,1)}), bf16[2048,1408]{1,0:T(8,128)(2,1)}) %all-gather.4.cloned.1.call-update) | async-done | bytes 5767184 | tf_op jit(solution)/shard_map/all_gather | solution.py:87
  222.8 5.2 %convolution_convert_fusion.4 = bf16[384,1408]{1,0:T(8,128)(2,1)S(1)} fusion(bf16[384,2048]{1,0:T(8,128)(2,1)S(1)} %constant_dynamic-update-slice_fusion.4, bf16[2048,1408]{1,0:T(8,128)(2,1)} %all-gather.4.cloned.1.call-done), kind=kOutput, calls=%fused_computation.14 | convolution fusion | flops 2215133184 | bytes 8421376 | tf_op jit(solution)/shard_map/dot_general | solution.py:154
  228.1 2.5 collective-permute-start.9
  230.6 0.1 fusion.49
  230.7 85.7 %all-gather.8.cloned.1.call-done = bf16[1408,2048]{1,0:T(8,128)(2,1)} async-done(((bf16[1408,256]{1,0:T(8,128)(2,1)}), bf16[1408,2048]{1,0:T(8,128)(2,1)}) %all-gather.8.cloned.1.call-update) | async-done | bytes 5767184 | tf_op jit(solution)/shard_map/all_gather | solution.py:88
  316.4 9.3 %convolution_convert_fusion.2 = bf16[384,2048]{1,0:T(8,128)(2,1)S(1)} fusion(bf16[1408,2048]{1,0:T(8,128)(2,1)} %all-gather.8.cloned.1.call-done, bf16[384,1408]{1,0:T(8,128)(2,1)} %copy-done.14, bf16[384,1408]{1,0:T(8,128)(2,1)} %copy-done.15, bf16[2,1408]{1,0:T(2,128)(2,1)S(1)} %collective-permute-done.11, ...), kind=kOutput, calls=%fused_computation.12 | convolution fusion | flops 2239168512 | bytes 9552384 | tf_op jit(solution)/shard_map/dot_general | solution.py:189
  325.7 0.1 slice_bitcast_fusion.3
  325.8 1.4 pad_maximum_fusion.1
  327.2 3.7 %all-to-all-start.1 = ((bf16[4,384,512]{2,1,0:T(8,128)(2,1)}), bf16[4,384,512]{2,1,0:T(8,128)(2,1)S(1)}, u32[]{:S(2)}, u32[]{:S(2)}) async-start(bf16[4,384,512]{2,1,0:T(8,128)(2,1)} %pad_maximum_fusion.1), calls=%async_computation.1 | async-start | bytes 3145728 | tf_op jit(solution)/shard_map/all_to_all | solution.py:49
  331.0 20.0 %all-to-all-done.1 = bf16[4,384,512]{2,1,0:T(8,128)(2,1)S(1)} async-done(((bf16[4,384,512]{2,1,0:T(8,128)(2,1)}), bf16[4,384,512]{2,1,0:T(8,128)(2,1)S(1)}, u32[]{:S(2)}, u32[]{:S(2)}) %all-to-all-start.1) | async-done | bytes 1572896 | tf_op jit(solution)/shard_map/all_to_all | solution.py:49
  350.9 0.2 convert_reduce_fusion
  351.2 1.2 fusion.37
  352.4 5.8 %all-reduce = (f32[384]{0:T(512)S(1)}, f32[384]{0:T(512)S(1)}) all-reduce(f32[384]{0:T(512)S(1)} %get-tuple-element.6, f32[384]{0:T(512)S(1)} %get-tuple-element.5), channel_id=1, replica_groups=mesh['sp'=8,'tp'=4] {'tp'}, use_global_device_ids=true, to_apply=%region_11.12 | all-reduce | flops 768 | bytes 6144 | tf_op jit(solution)/shard_map/psum | solution.py:192
  358.2 2.0 add_convert_fusion
  (63 shorter events, 0.3 us)
Async XLA Ops:
  6.5 55.0 %copy-start = (bf16[512,1024]{1,0:T(8,128)(2,1)S(1)}, bf16[512,1024]{1,0:T(8,128)(2,1)}, u32[]{:S(2)}) copy-start(bf16[512,1024]{1,0:T(8,128)(2,1)} %param.24) | copy-start | bytes 3145732
  6.5 19.7 %copy-start.6 = (bf16[384,512]{1,0:T(8,128)(2,1)S(1)}, bf16[384,512]{1,0:T(8,128)(2,1)}, u32[]{:S(2)}) copy-start(bf16[384,512]{1,0:T(8,128)(2,1)} %param.20) | copy-start | bytes 1179652
  6.5 167.2 %all-gather.6.cloned.1.call-start = ((), (), s32[]{:S(2)}) async-start(), calls=%async_computation.3 | async-start | bytes 6488064 | tf_op jit(solution)/shard_map/all_gather | solution.py:86
  7.3 19.3 %copy-start.5 = (bf16[384,512]{1,0:T(8,128)(2,1)S(1)}, bf16[384,512]{1,0:T(8,128)(2,1)}, u32[]{:S(2)}) copy-start(bf16[384,512]{1,0:T(8,128)(2,1)} %param.21) | copy-start | bytes 1179652
  7.3 26.6 %copy-start.7 = (s32[384]{0:T(512)S(1)}, s32[384]{0:T(512)}, u32[]{:S(2)}) copy-start(s32[384]{0:T(512)} %param.23) | copy-start | bytes 4612
  7.3 215.5 %all-gather.4.cloned.1.call-start = ((), (), s32[]{:S(2)}) async-start(), calls=%async_computation.2 | async-start | bytes 6488064 | tf_op jit(solution)/shard_map/all_gather | solution.py:87
  8.0 308.3 %all-gather.8.cloned.1.call-start = ((), (), s32[]{:S(2)}) async-start(), calls=%async_computation.4 | async-start | bytes 6488064 | tf_op jit(solution)/shard_map/all_gather | solution.py:88
  9.2 66.1 %collective-permute-start.6 = (bf16[384,64]{0,1:T(8,128)(2,1)S(1)}, bf16[384,64]{0,1:T(8,128)(2,1)S(1)}, u32[]{:S(2)}, u32[]{:S(2)}) collective-permute-start(bf16[384,64]{0,1:T(8,128)(2,1)S(1)} %pad_maximum_fusion.4), channel_id=1, source_target_pairs={{0,12},{4,16},{8,20},{12,24},{16,28},{1,13},{5,17},{9,21},{13,25},... | collective-permute-start | bytes 147464 | tf_op jit(solution)/shard_map/ppermute | solution.py:23
  15.1 60.2 %collective-permute-start.7 = (bf16[384,64]{0,1:T(8,128)(2,1)S(1)}, bf16[384,64]{0,1:T(8,128)(2,1)S(1)}, u32[]{:S(2)}, u32[]{:S(2)}) collective-permute-start(bf16[384,64]{0,1:T(8,128)(2,1)S(1)} %pad_maximum_fusion.4), channel_id=1, source_target_pairs={{0,8},{4,12},{8,16},{12,20},{16,24},{20,28},{1,9},{5,13},{9,17},{1... | collective-permute-start | bytes 147464 | tf_op jit(solution)/shard_map/ppermute | solution.py:23
  18.6 8.0 %collective-permute-start.3 = (s32[384]{0:T(512)}, s32[384]{0:T(512)S(1)}, u32[]{:S(2)}, u32[]{:S(2)}) collective-permute-start(s32[384]{0:T(512)} %param.23), channel_id=1, source_target_pairs={{0,12},{4,16},{8,20},{12,24},{16,28},{1,13},{5,17},{9,21},{13,25},... | collective-permute-start | bytes 4616 | tf_op jit(solution)/shard_map/ppermute | solution.py:23
  21.5 7.7 %collective-permute-start.4 = (s32[384]{0:T(512)}, s32[384]{0:T(512)S(1)}, u32[]{:S(2)}, u32[]{:S(2)}) collective-permute-start(s32[384]{0:T(512)} %param.23), channel_id=1, source_target_pairs={{0,8},{4,12},{8,16},{12,20},{16,24},{20,28},{1,9},{5,13},{9,17},{1... | collective-permute-start | bytes 4616 | tf_op jit(solution)/shard_map/ppermute | solution.py:23
  23.4 7.1 %collective-permute-start.5 = (s32[384]{0:T(512)}, s32[384]{0:T(512)S(1)}, u32[]{:S(2)}, u32[]{:S(2)}) collective-permute-start(s32[384]{0:T(512)} %param.23), channel_id=1, source_target_pairs={{0,4},{4,8},{8,12},{12,16},{16,20},{20,24},{24,28},{1,5},{5,9},{9,... | collective-permute-start | bytes 4616 | tf_op jit(solution)/shard_map/ppermute | solution.py:23
  26.6 20.5 %collective-permute-start = (bf16[384,512]{1,0:T(8,128)(2,1)S(1)}, bf16[384,512]{1,0:T(8,128)(2,1)S(1)}, u32[]{:S(2)}, u32[]{:S(2)}) collective-permute-start(bf16[384,512]{1,0:T(8,128)(2,1)S(1)} %copy-done.5), channel_id=1, source_target_pairs={{0,12},{4,16},{8,20},{12,24},{16,28},{1,13},{5,17},{9,21},{13,25},... | collective-permute-start | bytes 1179656 | tf_op jit(solution)/shard_map/ppermute | solution.py:23
  29.2 32.3 %collective-permute-start.1 = (bf16[384,512]{1,0:T(8,128)(2,1)S(1)}, bf16[384,512]{1,0:T(8,128)(2,1)S(1)}, u32[]{:S(2)}, u32[]{:S(2)}) collective-permute-start(bf16[384,512]{1,0:T(8,128)(2,1)S(1)} %copy-done.5), channel_id=1, source_target_pairs={{0,8},{4,12},{8,16},{12,20},{16,24},{20,28},{1,9},{5,13},{9,17},{1... | collective-permute-start | bytes 1179656 | tf_op jit(solution)/shard_map/ppermute | solution.py:23
  30.5 31.0 %collective-permute-start.2 = (bf16[384,512]{1,0:T(8,128)(2,1)S(1)}, bf16[384,512]{1,0:T(8,128)(2,1)S(1)}, u32[]{:S(2)}, u32[]{:S(2)}) collective-permute-start(bf16[384,512]{1,0:T(8,128)(2,1)S(1)} %copy-done.5), channel_id=1, source_target_pairs={{0,4},{4,8},{8,12},{12,16},{16,20},{20,24},{24,28},{1,5},{5,9},{9,... | collective-permute-start | bytes 1179656 | tf_op jit(solution)/shard_map/ppermute | solution.py:23
  47.1 28.3 %collective-permute-start.8 = (bf16[384,64]{0,1:T(8,128)(2,1)S(1)}, bf16[384,64]{0,1:T(8,128)(2,1)S(1)}, u32[]{:S(2)}, u32[]{:S(2)}) collective-permute-start(bf16[384,64]{0,1:T(8,128)(2,1)S(1)} %pad_maximum_fusion.4), channel_id=1, source_target_pairs={{0,4},{4,8},{8,12},{12,16},{16,20},{20,24},{24,28},{1,5},{5,9},{9,... | collective-permute-start | bytes 147464 | tf_op jit(solution)/shard_map/ppermute | solution.py:23
  61.6 1.9 copy-start.4
  63.5 8.3 %copy-start.16 = (bf16[512,1024]{1,0:T(8,128)(2,1)S(1)}, bf16[512,1024]{1,0:T(8,128)(2,1)}, u32[]{:S(2)}) copy-start(bf16[512,1024]{1,0:T(8,128)(2,1)} %param.25) | copy-start | bytes 3145732
  125.9 16.3 %copy-start.10 = (bf16[512]{0:T(512)(128)(2,1)S(1)}, bf16[512]{0:T(512)(128)(2,1)}, u32[]{:S(2)}) copy-start(bf16[512]{0:T(512)(128)(2,1)} %param.27) | copy-start | bytes 3076
  125.9 16.3 %copy-start.11 = (bf16[512]{0:T(512)(128)(2,1)S(1)}, bf16[512]{0:T(512)(128)(2,1)}, u32[]{:S(2)}) copy-start(bf16[512]{0:T(512)(128)(2,1)} %param.28) | copy-start | bytes 3076
  125.9 16.3 %copy-start.8 = (bf16[3,1408]{1,0:T(4,128)(2,1)S(1)}, bf16[3,1408]{1,0:T(4,128)(2,1)}, u32[]{:S(2)}) copy-start(bf16[3,1408]{1,0:T(4,128)(2,1)} %param.31) | copy-start | bytes 25348
  125.9 16.3 %copy-start.9 = (bf16[3,1408]{1,0:T(4,128)(2,1)S(1)}, bf16[3,1408]{1,0:T(4,128)(2,1)}, u32[]{:S(2)}) copy-start(bf16[3,1408]{1,0:T(4,128)(2,1)} %param.32) | copy-start | bytes 25348
  125.9 24.0 %copy-start.3 = (bf16[384,512]{1,0:T(8,128)(2,1)S(1)}, bf16[384,512]{1,0:T(8,128)(2,1)}, u32[]{:S(2)}) copy-start(bf16[384,512]{1,0:T(8,128)(2,1)} %param.18) | copy-start | bytes 1179652
  125.9 23.7 %all-to-all-start = ((bf16[4,384,512]{2,1,0:T(8,128)(2,1)}), bf16[4,384,512]{2,1,0:T(8,128)(2,1)S(1)}, u32[]{:S(2)}, u32[]{:S(2)}) async-start(bf16[4,384,512]{2,1,0:T(8,128)(2,1)} %pad_maximum_fusion), calls=%async_computation | async-start | bytes 3145728 | tf_op jit(solution)/shard_map/all_to_all | solution.py:49
  129.7 13.7 %collective-permute-start.10 = (s32[2]{0:T(128)S(1)}, s32[2]{0:T(128)S(1)}, u32[]{:S(2)}, u32[]{:S(2)}) collective-permute-start(s32[2]{0:T(128)S(1)} %slice.108), channel_id=1, source_target_pairs={{0,4},{4,8},{8,12},{12,16},{16,20},{20,24},{24,28},{1,5},{5,9},{9,... | collective-permute-start | bytes 32 | tf_op jit(solution)/shard_map/ppermute | solution.py:23
  156.5 17.2 %copy-start.2 = (bf16[384,512]{1,0:T(8,128)(2,1)}, bf16[384,512]{1,0:T(8,128)(2,1)S(1)}, u32[]{:S(2)}) copy-start(bf16[384,512]{1,0:T(8,128)(2,1)S(1)} %add_convert_fusion.1) | copy-start | bytes 1179652
  179.0 1.0 copy-start.14
  180.0 136.4 %collective-permute-start.11 = (bf16[2,1408]{1,0:T(2,128)(2,1)S(1)}, bf16[2,1408]{1,0:T(2,128)(2,1)S(1)}, u32[]{:S(2)}, u32[]{:S(2)}) collective-permute-start(bf16[2,1408]{1,0:T(2,128)(2,1)S(1)} %slice.137), channel_id=1, source_target_pairs={{0,4},{4,8},{8,12},{12,16},{16,20},{20,24},{24,28},{1,5},{5,9},{9,... | collective-permute-start | bytes 16904 | tf_op jit(solution)/shard_map/ppermute | solution.py:23
  228.0 2.5 copy-start.15
  228.1 88.3 %collective-permute-start.9 = (bf16[2,1408]{1,0:T(2,128)(2,1)S(1)}, bf16[2,1408]{1,0:T(2,128)(2,1)S(1)}, u32[]{:S(2)}, u32[]{:S(2)}) collective-permute-start(bf16[2,1408]{1,0:T(2,128)(2,1)S(1)} %slice.134), channel_id=1, source_target_pairs={{0,4},{4,8},{8,12},{12,16},{16,20},{20,24},{24,28},{1,5},{5,9},{9,... | collective-permute-start | bytes 16904 | tf_op jit(solution)/shard_map/ppermute | solution.py:23
  327.2 3.7 %copy-start.12 = (bf16[512]{0:T(512)(128)(2,1)S(1)}, bf16[512]{0:T(512)(128)(2,1)}, u32[]{:S(2)}) copy-start(bf16[512]{0:T(512)(128)(2,1)} %param.34) | copy-start | bytes 3076
  327.2 3.7 %copy-start.13 = (bf16[512]{0:T(512)(128)(2,1)S(1)}, bf16[512]{0:T(512)(128)(2,1)}, u32[]{:S(2)}) copy-start(bf16[512]{0:T(512)(128)(2,1)} %param.35) | copy-start | bytes 3076
  327.2 23.7 %all-to-all-start.1 = ((bf16[4,384,512]{2,1,0:T(8,128)(2,1)}), bf16[4,384,512]{2,1,0:T(8,128)(2,1)S(1)}, u32[]{:S(2)}, u32[]{:S(2)}) async-start(bf16[4,384,512]{2,1,0:T(8,128)(2,1)} %pad_maximum_fusion.1), calls=%async_computation.1 | async-start | bytes 3145728 | tf_op jit(solution)/shard_map/all_to_all | solution.py:49
  330.9 29.2 %copy-start.1 = (bf16[512,1024]{1,0:T(8,128)(2,1)S(1)}, bf16[512,1024]{1,0:T(8,128)(2,1)}, u32[]{:S(2)}) copy-start(bf16[512,1024]{1,0:T(8,128)(2,1)} %param.24) | copy-start | bytes 3145732
Sparse Core Ops, SparseCore 0:
  9.5 118.1 all-gather.5
  129.9 92.8 all-gather.3
  224.8 91.4 all-gather.7

commit v2 on v1

--- a/solution.py
+++ b/solution.py
@@ -1,6 +1,10 @@
+import functools
+
 import jax
 import jax.numpy as jnp
 from jax import lax
+from jax.experimental import pallas as pl
+from jax.experimental.pallas import tpu as pltpu
 from jax.sharding import PartitionSpec as P
 
 D = 2048
@@ -40,6 +44,75 @@
         ],
         axis=-1,
     )
+
+
+def ring_blocks(block, axis):
+    count = lax.axis_size(axis)
+    order = list(range(0, count, 2)) + list(range(1, count, 2))[::-1]
+    place = [order.index(i) for i in range(count)]
+    me = lax.axis_index(axis)
+    found = [(me, block)]
+    ahead = count // 2
+    for turn, steps in ((1, ahead), (-1, count - 1 - ahead)):
+        pairs = [(order[p], order[(p + turn) % count]) for p in range(count)]
+        moving = block
+        for step in range(1, steps + 1):
+            moving = lax.ppermute(moving, axis, pairs)
+            owners = [order[(place[i] - turn * step) % count] for i in range(count)]
+            found.append((jnp.asarray(owners, jnp.int32)[me], moving))
+    return found
+
+
+def attend_kernel(chunk, reach_rows, scale, q_ref, turned_ref, k_ref, rope_ref, v_ref, bias_ref, out_ref):
+    rows = q_ref.shape[0]
+    span = chunk + reach_rows
+    rope_rows = rope_ref[...]
+    for head in range(q_ref.shape[1] // NOPE):
+        nope = slice(head * NOPE, (head + 1) * NOPE)
+        rope = slice(head * ROPE, (head + 1) * ROPE)
+        queries = jnp.concatenate([q_ref[:, nope], turned_ref[:, rope]], 1)
+        keys = jnp.concatenate([k_ref[:, nope], rope_rows], 1)
+        for start in range(0, rows, chunk):
+            cut = slice(start, start + chunk)
+            seen = slice(start, start + span)
+            scores = lax.dot_general(
+                queries[cut], keys[seen], (((1,), (1,)), ((), ())), preferred_element_type=jnp.float32
+            )
+            scores = scores * scale + bias_ref[cut, seen]
+            weights = jnp.exp(scores - jnp.max(scores, -1, keepdims=True))
+            weights = weights * (1.0 / jnp.sum(weights, -1, keepdims=True))
+            out_ref[cut, nope] = jnp.dot(
+                weights.astype(jnp.bfloat16), v_ref[seen, nope], preferred_element_type=jnp.float32
+            ).astype(jnp.bfloat16)
+
+
+def attend(queries, turned, keys, rope_rows, values, bias, scale):
+    rows, width = queries.shape
+    window = keys.shape[0]
+    chunk = 128 if rows % 128 == 0 else rows
+    pair = 2
+    wide = pair * NOPE
+    heads = width // NOPE
+    return pl.pallas_call(
+        functools.partial(attend_kernel, chunk, window - rows, scale),
+        grid=(heads // pair,),
+        in_specs=[
+            pl.BlockSpec((rows, wide), lambda i: (0, i)),
+            pl.BlockSpec((rows, pair * ROPE), lambda i: (0, i)),
+            pl.BlockSpec((window, wide), lambda i: (0, i)),
+            pl.BlockSpec((window, ROPE), lambda i: (0, 0)),
+            pl.BlockSpec((window, pair * VDIM), lambda i: (0, i)),
+            pl.BlockSpec((rows, window), lambda i: (0, 0)),
+        ],
+        out_specs=pl.BlockSpec((rows, pair * VDIM), lambda i: (0, i)),
+        out_shape=jax.ShapeDtypeStruct((rows, heads * VDIM), jnp.bfloat16),
+        compiler_params=pltpu.CompilerParams(vmem_limit_bytes=40 * 1024 * 1024),
+        cost_estimate=pl.CostEstimate(
+            flops=16 * rows * window * heads * (NOPE + ROPE + VDIM),
+            bytes_accessed=2 * (4 * rows * width + 2 * window * width),
+            transcendentals=rows * window * heads,
+        ),
+    )(queries, turned, keys, rope_rows, values, bias)
 
 
 def scatter_sum(terms, axis):
@@ -82,11 +155,8 @@
     head_count = query_nope.shape[1] // NOPE
     local_units = ffn_gate.shape[1]
     rim_rows = CONV - 1
-    whole_gate, whole_value, whole_down = (
-        lax.all_gather(ffn_gate, "sp", axis=0, tiled=True),
-        lax.all_gather(ffn_value, "sp", axis=0, tiled=True),
-        lax.all_gather(ffn_down, "sp", axis=1, tiled=True),
-    )
+    whole_gate = lax.all_gather(ffn_gate, "sp", axis=0, tiled=True)
+    whole_value = lax.all_gather(ffn_value, "sp", axis=0, tiled=True)
     offset = lax.axis_index("sp") * row_count
     positions = offset + jnp.arange(row_count, dtype=jnp.int32)
     cosine, sine_table = tables(positions)
@@ -96,17 +166,21 @@
         cosine[:, None],
         sine_table[:, None],
     ).astype(jnp.bfloat16)
-    latent_list = []
-    rim_list = []
-    doc_list = []
-    for shift_step in range(REACH, 0, -1):
-        far_latent, far_key, far_doc = passed_along((latent, turned_key, doc_ids), "sp", shift_step)
-        latent_list.append(far_latent)
-        rim_list.append(far_key)
-        doc_list.append(far_doc)
-    win_latent = jnp.concatenate(latent_list + [latent], 0)
-    win_key = jnp.concatenate(rim_list + [turned_key], 0)
-    win_doc = jnp.concatenate(doc_list + [doc_ids], 0)
+    latent_width = latent.shape[1]
+    packed = jnp.concatenate(
+        [
+            latent,
+            turned_key,
+            jnp.broadcast_to(doc_ids.astype(jnp.bfloat16)[:, None], (row_count, ROPE)),
+        ],
+        1,
+    )
+    parts = [passed_along(packed, "sp", shift_step) for shift_step in range(REACH, 0, -1)]
+    pieces = jnp.concatenate(parts + [packed], 0)
+    win_latent = pieces[:, :latent_width]
+    win_key = pieces[:, latent_width : latent_width + ROPE]
+    win_doc = pieces[:, latent_width + ROPE].astype(jnp.int32)
+    down_blocks = ring_blocks(ffn_down, "sp")
     key_rows = jnp.dot(win_latent, key_up, preferred_element_type=jnp.float32).astype(jnp.bfloat16)
     values = jnp.dot(win_latent, value_up, preferred_element_type=jnp.float32).astype(jnp.bfloat16)
     window = key_rows.shape[0]
@@ -117,26 +191,16 @@
         & (win_doc[None, :] == doc_ids[:, None])
     )
     scale = (NOPE + ROPE) ** (-0.5)
-    scores = jnp.einsum(
-        "qhd,khd->hqk",
-        query_nope.reshape(row_count, head_count, NOPE),
-        key_rows.reshape(window, head_count, NOPE),
-        preferred_element_type=jnp.float32,
-    )
-    scores = scores + jnp.einsum(
-        "qhr,kr->hqk", turned_query, win_key, preferred_element_type=jnp.float32
-    )
-    scores = jnp.where(allowed[None], scores * scale, masked_score)
-    row_max = jnp.max(scores, -1, keepdims=True)
-    weights = jnp.exp(scores - row_max)
-    weights = (weights / jnp.sum(weights, -1, keepdims=True)).astype(jnp.bfloat16)
-    attended = jnp.einsum(
-        "hqk,khd->qhd",
-        weights,
-        values.reshape(window, head_count, VDIM),
-        preferred_element_type=jnp.float32,
-    )
-    attended = attended.astype(jnp.bfloat16).reshape(row_count, head_count * VDIM)
+    bias = jnp.where(allowed, 0.0, masked_score).astype(jnp.float32)
+    attended = attend(
+        query_nope,
+        turned_query.reshape(row_count, head_count * ROPE),
+        key_rows,
+        win_key,
+        values,
+        bias,
+        scale,
+    )
     head_terms = jnp.dot(attended, out_proj, preferred_element_type=jnp.float32)
     projected = scatter_sum(head_terms, "tp")
     mixed_one = residual_scale * residual.astype(jnp.float32) + projected
@@ -186,8 +250,19 @@
             * valid_tap
         )
     hidden = (value_mix * jax.nn.gelu(gate_mix)).astype(jnp.bfloat16)
-    unit_terms = jnp.dot(hidden, whole_down, preferred_element_type=jnp.float32)
-    ffn_out = scatter_sum(unit_terms, "tp")
+    sp_count = lax.axis_size("sp")
+    tp_count = lax.axis_size("tp")
+    block_width = ffn_down.shape[1]
+    unit_terms = jnp.zeros((sp_count, row_count, block_width), jnp.bfloat16)
+    for owner, block in down_blocks:
+        term = jnp.dot(hidden, block, preferred_element_type=jnp.float32).astype(jnp.bfloat16)
+        unit_terms = lax.dynamic_update_slice(unit_terms, term[None], (owner, 0, 0))
+    share = sp_count // tp_count
+    got = lax.all_to_all(
+        unit_terms.reshape(tp_count, share, row_count, block_width), "tp", 0, 0
+    )
+    ffn_blocks = jnp.sum(got.astype(jnp.float32), 0)
+    ffn_out = jnp.concatenate([ffn_blocks[i] for i in range(share)], 1)
     mixed_two = residual_scale * normed.astype(jnp.float32) + ffn_out
     totals_two = lax.psum((jnp.sum(mixed_two, 1), jnp.sum(mixed_two * mixed_two, 1)), "tp")
     return finish(mixed_two, totals_two, norm2_gain, norm2_bias).astype(jnp.bfloat16)

time: 368 us -> 330 us (0.90)
  waiting for transfers between devices: 167 us -> 86.7 us
  starting transfers between devices: 62.4 us -> 103 us
  matrix products: 67.2 us -> 27.3 us
  Pallas kernels: 0 us -> 17.2 us
  between operations: 13.7 us -> 26.9 us
  local copies, waits for them, and re-layouts: 1.76 us -> 13.7 us
    all_gather x3 -> x2, waiting for transfers between devices: 116 us -> 27.2 us  [the longest x1 27.2 us: local(): whole_value = lax.all_gather(ffn_value, 'sp', axis=0, tiled=True)]
    dot_general x4 -> x8, matrix products: 47.3 us -> 10.5 us  [local(): jnp.dot(hidden, block, preferred_element_type=jnp.float32)]
    ppermute x0 -> x7, starting transfers between devices: none -> 27.2 us  [ring_blocks(): moving = lax.ppermute(moving, axis, pairs)]
    all_to_all x2 -> x1, waiting for transfers between devices: 26.1 us -> 0.01 us  [scatter_sum(): got = lax.all_to_all(parts.astype(jnp.bfloat16), axis, 0, 0)]
    all_to_all x0 -> x1, waiting for transfers between devices: none -> 20 us  [local(): lax.all_to_all(unit_terms.reshape(tp_count, share, row_count, block_width...]
    pallas_call x0 -> x1, Pallas kernels: none -> 17.2 us  [attend(): pl.pallas_call(functools.partial(attend_kernel, chunk, window - rows, sca...]
    sub x1 -> x0, other arithmetic: 15.4 us -> none  [local(): weights = jnp.exp(scores - row_max)]
    ppermute x12 -> x6, starting transfers between devices: 55 us -> 68.2 us  [passed_along(): return lax.ppermute(value, axis, pairs)]
  transfers between devices with their start and end apart: 17 -> 17, of which waited for: 7 -> 6; matrix products, arithmetic and copies ran while one was open for 22% -> 19% of each run, Pallas kernels for 0% -> 5%
where the time goes in v2:
time: 330 us; the launch traced here: 329 us
  starting transfers between devices  103 us (31%)
  waiting for transfers between devices  86.7 us (26%)
  blocking collectives  29.7 us (9%)
  matrix products  27.3 us (8%)
  between operations  26.9 us (8%)
  other arithmetic  24.5 us (7%)
  Pallas kernels  17.2 us (5%)
  local copies, waits for them, and re-layouts  13.7 us (4%)
    ppermute x6, starting transfers between devices, passed_along(): return lax.ppermute(value, axis, pairs)  68.2 us
    ppermute x6, waiting for transfers between devices, passed_along(): return lax.ppermute(value, axis, pairs)  31.2 us
    ppermute x7, starting transfers between devices, ring_blocks(): moving = lax.ppermute(moving, axis, pairs)  27.2 us
    all_gather x1, waiting for transfers between devices, local(): whole_value = lax.all_gather(ffn_value, 'sp', axis=0, tiled=True)  27.2 us
    all_to_all x1, waiting for transfers between devices, local(): lax.all_to_all(unit_terms.reshape(tp_count, share, row_count, block_width...  20 us
    pallas_call x1, Pallas kernels, attend(): pl.pallas_call(functools.partial(attend_kernel, chunk, window - rows, sca...  17.2 us
    dot_general x8, matrix products, local(): jnp.dot(hidden, block, preferred_element_type=jnp.float32)  10.5 us
    all_gather x1, blocking collectives, local(): lax.all_gather(normed[:half], 'tp', axis=1, tiled=True)  9.22 us
  transfers between devices with their start and end apart: 17, of which 6 were waited for; matrix products, arithmetic and copies ran while one was open for 19% of the time, Pallas kernels for 5%

profile of v2, /device:TPU:0, one launch (start us, length us, event | category | flops | bytes accessed | tf_op | source)
XLA Modules:
  0.0 328.8 jit_solution(16483978702596401627)
XLA Ops:
  6.5 0.7 all-gather.5.cloned.1.call-update
  7.3 0.7 all-gather.3.cloned.1.call-update
  8.0 0.9 copy.36
  9.0 0.7 convert_element_type.147
  9.7 1.6 subtract_convert_fusion.1
  11.4 0.9 pad_maximum_fusion.3
  12.3 4.9 %collective-permute-start.2 = (bf16[384,640]{1,0:T(8,128)(2,1)}, bf16[384,640]{1,0:T(8,128)(2,1)S(1)}, u32[]{:S(2)}, u32[]{:S(2)}) collective-permute-start(bf16[384,640]{1,0:T(8,128)(2,1)} %pad_maximum_fusion.3), channel_id=1, source_target_pairs={{0,4},{4,8},{8,12},{12,16},{16,20},{20,24},{24,28},{1,5},{5,9},{9,... | collective-permute-start | bytes 1474568 | tf_op jit(solution)/shard_map/ppermute | solution.py:27
  17.2 3.5 %collective-permute-start.1 = (bf16[384,640]{1,0:T(8,128)(2,1)}, bf16[384,640]{1,0:T(8,128)(2,1)S(1)}, u32[]{:S(2)}, u32[]{:S(2)}) collective-permute-start(bf16[384,640]{1,0:T(8,128)(2,1)} %pad_maximum_fusion.3), channel_id=1, source_target_pairs={{0,8},{4,12},{8,16},{12,20},{16,24},{20,28},{1,9},{5,13},{9,17},{1... | collective-permute-start | bytes 1474568 | tf_op jit(solution)/shard_map/ppermute | solution.py:27
  20.7 4.5 %collective-permute-start = (bf16[384,640]{1,0:T(8,128)(2,1)}, bf16[384,640]{1,0:T(8,128)(2,1)S(1)}, u32[]{:S(2)}, u32[]{:S(2)}) collective-permute-start(bf16[384,640]{1,0:T(8,128)(2,1)} %pad_maximum_fusion.3), channel_id=1, source_target_pairs={{0,12},{4,16},{8,20},{12,24},{16,28},{1,13},{5,17},{9,21},{13,25},... | collective-permute-start | bytes 1474568 | tf_op jit(solution)/shard_map/ppermute | solution.py:27
  25.3 1.2 copy.32
  26.5 1.0 convert.39
  27.4 1.0 copy.35
  28.5 1.0 copy.34
  29.5 1.2 subtract_convert_fusion
  30.7 0.8 pad_maximum_fusion.4
  31.5 1.2 copy.37.turned_ref
  32.8 2.9 collective-permute-done.2
  35.7 7.1 %collective-permute-done.1 = bf16[384,640]{1,0:T(8,128)(2,1)S(1)} collective-permute-done((bf16[384,640]{1,0:T(8,128)(2,1)}, bf16[384,640]{1,0:T(8,128)(2,1)S(1)}, u32[]{:S(2)}, u32[]{:S(2)}) %collective-permute-start.1) | collective-permute-done | bytes 491552 | tf_op jit(solution)/shard_map/ppermute | solution.py:27
  42.9 21.1 %collective-permute-done = bf16[384,640]{1,0:T(8,128)(2,1)S(1)} collective-permute-done((bf16[384,640]{1,0:T(8,128)(2,1)}, bf16[384,640]{1,0:T(8,128)(2,1)S(1)}, u32[]{:S(2)}, u32[]{:S(2)}) %collective-permute-start) | collective-permute-done | bytes 491552 | tf_op jit(solution)/shard_map/ppermute | solution.py:27
  63.9 1.3 convert_reduce_fusion.2
  65.4 7.1 %maximum_maximum_fusion = bf16[1536,640]{1,0:T(8,128)(2,1)S(1)} fusion(bf16[384,64]{1,0:T(8,128)(2,1)S(1)} %copy-done.7, bf16[384,32]{1,0:T(8,128)(2,1)S(1)} %get-tuple-element.30, bf16[384,32]{1,0:T(8,128)(2,1)S(1)} %get-tuple-element.29, bf16[384,512]{1,0:T(8,128)(2,1)S(1)} %copy-done.5, bf16[384,640]{1,0:T(8,128)(2,1)S(1)} %collective-permute-done.2, ...), kind=kLoop, calls=%fused_computation.18 | loop fusion | flops 13762560 | bytes 3932160 | tf_op jit(solution)/shard_map/concatenate | solution.py:179
  72.5 1.8 convolution_convert_fusion.1.k_ref
  74.4 1.8 convolution_convert_fusion.v_ref
  76.2 0.7 and_select_fusion.bias_ref
  77.3 17.2 %shard_map.235 = bf16[384,1024]{1,0:T(8,128)(2,1)S(1)} custom-call(bf16[384,1024]{1,0:T(8,128)(2,1)S(1)} %copy-done.1, bf16[384,512]{1,0:T(8,128)(2,1)S(1)} %copy.37.turned_ref, bf16[1536,1024]{1,0:T(8,128)(2,1)S(1)} %convolution_convert_fusion.1.k_ref, bf16[1536,64]{1,0:T(8,128)(2,1)S(1)} %maximum_maximum_fusion.1.rope_ref, ...), custom_call_target="tpu_custom_call" | custom-call | flops 24159191040 | bytes 9437184 | tf_op jit(solution)/shard_map/pallas_call | solution.py:96
  94.5 1.8 convolution_convert_fusion.4
  96.4 1.4 pad_maximum_fusion
  98.0 3.7 %all-to-all-start = ((bf16[4,384,512]{2,1,0:T(8,128)(2,1)}), bf16[4,384,512]{2,1,0:T(8,128)(2,1)S(1)}, u32[]{:S(2)}, u32[]{:S(2)}) async-start(bf16[4,384,512]{2,1,0:T(8,128)(2,1)} %pad_maximum_fusion), calls=%async_computation | async-start | bytes 3145728 | tf_op jit(solution)/shard_map/all_to_all | solution.py:122
  101.7 9.9 %collective-permute-start.10 = (bf16[1408,256]{1,0:T(8,128)(2,1)}, bf16[1408,256]{1,0:T(8,128)(2,1)}, u32[]{:S(2)}, u32[]{:S(2)}) collective-permute-start(bf16[1408,256]{1,0:T(8,128)(2,1)} %param.40), channel_id=1, source_target_pairs={{0,4},{8,0},{16,8},{24,16},{28,24},{20,28},{12,20},{4,12},{1,5},{9... | collective-permute-start | bytes 2162696 | tf_op jit(solution)/shard_map/ppermute | solution.py:60
  111.7 42.0 %collective-permute-start.4 = (s32[2]{0:T(128)S(1)}, s32[2]{0:T(128)S(1)}, u32[]{:S(2)}, u32[]{:S(2)}) collective-permute-start(s32[2]{0:T(128)S(1)} %slice.110), channel_id=1, source_target_pairs={{0,4},{4,8},{8,12},{12,16},{16,20},{20,24},{24,28},{1,5},{5,9},{9,... | collective-permute-start | bytes 32 | tf_op jit(solution)/shard_map/ppermute | solution.py:27
  153.7 0.6 dynamic_slice.21
  155.6 0.6 dynamic_slice.22
  157.5 0.6 dynamic_slice.23
  161.0 0.6 dynamic_slice.25
  162.9 0.6 dynamic_slice.26
  164.8 0.6 dynamic_slice.27
  171.0 11.8 %collective-permute-start.11 = (bf16[1408,256]{1,0:T(8,128)(2,1)}, bf16[1408,256]{1,0:T(8,128)(2,1)}, u32[]{:S(2)}, u32[]{:S(2)}) collective-permute-start(bf16[1408,256]{1,0:T(8,128)(2,1)} %collective-permute-done.10), channel_id=1, source_target_pairs={{0,4},{8,0},{16,8},{24,16},{28,24},{20,28},{12,20},{4,12},{1,5},{9... | collective-permute-start | bytes 2162696 | tf_op jit(solution)/shard_map/ppermute | solution.py:60
  182.9 1.9 collective-permute-start.8
  185.0 1.2 fusion.29
  186.2 6.1 %all-reduce.1 = (f32[384]{0:T(512)S(1)}, f32[384]{0:T(512)S(1)}) all-reduce(f32[384]{0:T(512)S(1)} %get-tuple-element.8, f32[384]{0:T(512)S(1)} %get-tuple-element.7), channel_id=1, replica_groups=mesh['sp'=8,'tp'=4] {'tp'}, use_global_device_ids=true, to_apply=%region_4.5 | all-reduce | flops 768 | bytes 6144 | tf_op jit(solution)/shard_map/psum | solution.py:207
  192.3 1.2 add_convert_fusion.1
  193.6 9.2 %all_gather.12 = bf16[192,2048]{1,0:T(8,128)(2,1)S(1)} all-gather(bf16[192,512]{1,0:T(8,128)(2,1)S(1)} %get-tuple-element.28), channel_id=1, replica_groups=mesh['sp'=8,'tp'=4] {'tp'}, dimensions={1}, use_global_device_ids=true | all-gather | bytes 983040 | tf_op jit(solution)/shard_map/all_gather | solution.py:212
  202.8 1.0 constant_dynamic-update-slice_fusion.1
  203.8 8.7 %all_gather.13 = bf16[192,2048]{1,0:T(8,128)(2,1)S(1)} all-gather(bf16[192,512]{1,0:T(8,128)(2,1)S(1)} %get-tuple-element.27), channel_id=1, replica_groups=mesh['sp'=8,'tp'=4] {'tp'}, dimensions={1}, use_global_device_ids=true | all-gather | bytes 983040 | tf_op jit(solution)/shard_map/all_gather | solution.py:213
  212.5 1.0 constant_dynamic-update-slice_fusion
  213.5 5.7 %convolution_convert_fusion.2 = bf16[384,1408]{1,0:T(8,128)(2,1)S(1)} fusion(bf16[384,2048]{1,0:T(8,128)(2,1)} %constant_dynamic-update-slice_fusion, bf16[2048,1408]{1,0:T(8,128)(2,1)} %all-gather.5.cloned.1.call-done), kind=kOutput, calls=%fused_computation.5 | convolution fusion | flops 2215133184 | bytes 8421376 | tf_op jit(solution)/shard_map/dot_general | solution.py:217
  219.2 10.1 %collective-permute-start.5 = (bf16[2,1408]{1,0:T(2,128)(2,1)S(1)}, bf16[2,1408]{1,0:T(2,128)(2,1)S(1)}, u32[]{:S(2)}, u32[]{:S(2)}) collective-permute-start(bf16[2,1408]{1,0:T(2,128)(2,1)S(1)} %slice.138), channel_id=1, source_target_pairs={{0,4},{4,8},{8,12},{12,16},{16,20},{20,24},{24,28},{1,5},{5,9},{9,... | collective-permute-start | bytes 16904 | tf_op jit(solution)/shard_map/ppermute | solution.py:27
  229.3 27.2 %all-gather.3.cloned.1.call-done = bf16[2048,1408]{1,0:T(8,128)(2,1)} async-done(((bf16[256,1408]{1,0:T(8,128)(2,1)}), bf16[2048,1408]{1,0:T(8,128)(2,1)}) %all-gather.3.cloned.1.call-update) | async-done | bytes 5767184 | tf_op jit(solution)/shard_map/all_gather | solution.py:159
  256.5 5.7 %convolution_convert_fusion.3 = bf16[384,1408]{1,0:T(8,128)(2,1)S(1)} fusion(bf16[384,2048]{1,0:T(8,128)(2,1)} %constant_dynamic-update-slice_fusion, bf16[2048,1408]{1,0:T(8,128)(2,1)} %all-gather.3.cloned.1.call-done), kind=kOutput, calls=%fused_computation.6 | convolution fusion | flops 2215133184 | bytes 8421376 | tf_op jit(solution)/shard_map/dot_general | solution.py:218
  262.2 3.2 collective-permute-start.3
  265.5 3.0 collective-permute-start.12
  269.0 3.2 fusion.8
  272.3 1.6 fusion.12
  273.9 1.6 fusion.14
  275.5 1.6 fusion.16
  277.1 1.6 fusion.18
  278.7 7.0 %collective-permute-done.9 = bf16[1408,256]{1,0:T(8,128)(2,1)S(1)} collective-permute-done((bf16[1408,256]{1,0:T(8,128)(2,1)}, bf16[1408,256]{1,0:T(8,128)(2,1)S(1)}, u32[]{:S(2)}, u32[]{:S(2)}) %collective-permute-start.9) | collective-permute-done | bytes 720928 | tf_op jit(solution)/shard_map/ppermute | solution.py:60
  286.1 1.6 fusion.22
  287.7 1.6 fusion.24
  289.8 1.2 copy-done.2
  291.0 3.7 %all-to-all-start.1 = ((bf16[4,2,384,256]{3,2,1,0:T(8,128)(2,1)}), bf16[4,2,384,256]{3,2,1,0:T(8,128)(2,1)S(1)}, u32[]{:S(2)}, u32[]{:S(2)}) async-start(bf16[4,2,384,256]{3,2,1,0:T(8,128)(2,1)} %bitcast.79), calls=%async_computation.1 | async-start | bytes 3145728 | tf_op jit(solution)/shard_map/all_to_all | solution.py:261
  294.7 20.0 %all-to-all-done.1 = bf16[4,2,384,256]{3,2,1,0:T(8,128)(2,1)S(1)} async-done(((bf16[4,2,384,256]{3,2,1,0:T(8,128)(2,1)}), bf16[4,2,384,256]{3,2,1,0:T(8,128)(2,1)S(1)}, u32[]{:S(2)}, u32[]{:S(2)}) %all-to-all-start.1) | async-done | bytes 1572896 | tf_op jit(solution)/shard_map/all_to_all | solution.py:261
  315.2 5.8 %all-reduce = (f32[384]{0:T(512)S(1)}, f32[384]{0:T(512)S(1)}) all-reduce(f32[384]{0:T(512)S(1)} %get-tuple-element.6, f32[384]{0:T(512)S(1)} %get-tuple-element.5), channel_id=1, replica_groups=mesh['sp'=8,'tp'=4] {'tp'}, use_global_device_ids=true, to_apply=%region_9.10 | all-reduce | flops 768 | bytes 6144 | tf_op jit(solution)/shard_map/psum | solution.py:267
  321.0 1.0 add_convert_fusion
  (94 shorter events, 4.3 us)
Async XLA Ops:
  6.5 66.0 %copy-start = (bf16[512,1024]{1,0:T(8,128)(2,1)S(1)}, bf16[512,1024]{1,0:T(8,128)(2,1)}, u32[]{:S(2)}) copy-start(bf16[512,1024]{1,0:T(8,128)(2,1)} %param.31) | copy-start | bytes 3145732
  6.5 4.8 %copy-start.5 = (bf16[384,512]{1,0:T(8,128)(2,1)S(1)}, bf16[384,512]{1,0:T(8,128)(2,1)}, u32[]{:S(2)}) copy-start(bf16[384,512]{1,0:T(8,128)(2,1)} %param.28) | copy-start | bytes 1179652
  6.5 206.9 %all-gather.5.cloned.1.call-start = ((), (), s32[]{:S(2)}) async-start(), calls=%async_computation.3 | async-start | bytes 6488064 | tf_op jit(solution)/shard_map/all_gather | solution.py:158
  7.3 249.2 %all-gather.3.cloned.1.call-start = ((), (), s32[]{:S(2)}) async-start(), calls=%async_computation.2 | async-start | bytes 6488064 | tf_op jit(solution)/shard_map/all_gather | solution.py:159
  11.4 5.9 %copy-start.6 = (bf16[384,64]{1,0:T(8,128)(2,1)}, bf16[384,64]{1,0:T(8,128)(2,1)S(1)}, u32[]{:S(2)}) copy-start(bf16[384,64]{1,0:T(8,128)(2,1)S(1)} %broadcast_in_dim.28) | copy-start | bytes 147460
  12.3 23.4 %collective-permute-start.2 = (bf16[384,640]{1,0:T(8,128)(2,1)}, bf16[384,640]{1,0:T(8,128)(2,1)S(1)}, u32[]{:S(2)}, u32[]{:S(2)}) collective-permute-start(bf16[384,640]{1,0:T(8,128)(2,1)} %pad_maximum_fusion.3), channel_id=1, source_target_pairs={{0,4},{4,8},{8,12},{12,16},{16,20},{20,24},{24,28},{1,5},{5,9},{9,... | collective-permute-start | bytes 1474568 | tf_op jit(solution)/shard_map/ppermute | solution.py:27
  17.2 25.6 %collective-permute-start.1 = (bf16[384,640]{1,0:T(8,128)(2,1)}, bf16[384,640]{1,0:T(8,128)(2,1)S(1)}, u32[]{:S(2)}, u32[]{:S(2)}) collective-permute-start(bf16[384,640]{1,0:T(8,128)(2,1)} %pad_maximum_fusion.3), channel_id=1, source_target_pairs={{0,8},{4,12},{8,16},{12,20},{16,24},{20,28},{1,9},{5,13},{9,17},{1... | collective-permute-start | bytes 1474568 | tf_op jit(solution)/shard_map/ppermute | solution.py:27
  20.7 43.2 %collective-permute-start = (bf16[384,640]{1,0:T(8,128)(2,1)}, bf16[384,640]{1,0:T(8,128)(2,1)S(1)}, u32[]{:S(2)}, u32[]{:S(2)}) collective-permute-start(bf16[384,640]{1,0:T(8,128)(2,1)} %pad_maximum_fusion.3), channel_id=1, source_target_pairs={{0,12},{4,16},{8,20},{12,24},{16,28},{1,13},{5,17},{9,21},{13,25},... | collective-permute-start | bytes 1474568 | tf_op jit(solution)/shard_map/ppermute | solution.py:27
  25.2 86.4 %collective-permute-start.6 = (bf16[1408,256]{1,0:T(8,128)(2,1)}, bf16[1408,256]{1,0:T(8,128)(2,1)}, u32[]{:S(2)}, u32[]{:S(2)}) collective-permute-start(bf16[1408,256]{1,0:T(8,128)(2,1)} %param.40), channel_id=1, source_target_pairs={{0,8},{8,16},{16,24},{24,28},{28,20},{20,12},{12,4},{4,0},{1,9},{9... | collective-permute-start | bytes 2162696 | tf_op jit(solution)/shard_map/ppermute | solution.py:60
  32.7 32.5 %copy-start.7 = (bf16[384,64]{1,0:T(8,128)(2,1)S(1)}, bf16[384,64]{1,0:T(8,128)(2,1)}, u32[]{:S(2)}) copy-start(bf16[384,64]{1,0:T(8,128)(2,1)} %copy-done.6) | copy-start | bytes 147460
  72.5 1.8 copy-start.16
  74.4 1.8 copy-start.8
  76.2 1.1 copy-start.1
  77.3 17.2 %copy-start.15 = (bf16[1024,2048]{1,0:T(8,128)(2,1)S(1)}, bf16[1024,2048]{1,0:T(8,128)(2,1)}, u32[]{:S(2)}) copy-start(bf16[1024,2048]{1,0:T(8,128)(2,1)} %param.33) | copy-start | bytes 12582916
  97.9 55.8 %copy-start.23 = (s32[8]{0:T(128)S(1)}, s32[8]{0:T(128)}, u32[]{:S(2)}) copy-start(s32[8]{0:T(128)} %constant.70.clone) | copy-start | bytes 100
  97.9 57.7 %copy-start.22 = (s32[8]{0:T(128)S(1)}, s32[8]{0:T(128)}, u32[]{:S(2)}) copy-start(s32[8]{0:T(128)} %constant.71.clone) | copy-start | bytes 100
  97.9 59.6 %copy-start.21 = (s32[8]{0:T(128)S(1)}, s32[8]{0:T(128)}, u32[]{:S(2)}) copy-start(s32[8]{0:T(128)} %constant.72.clone) | copy-start | bytes 100
  97.9 61.5 %copy-start.20 = (s32[8]{0:T(128)S(1)}, s32[8]{0:T(128)}, u32[]{:S(2)}) copy-start(s32[8]{0:T(128)} %constant.73.clone) | copy-start | bytes 100
  97.9 63.1 %copy-start.19 = (s32[8]{0:T(128)S(1)}, s32[8]{0:T(128)}, u32[]{:S(2)}) copy-start(s32[8]{0:T(128)} %constant.74.clone) | copy-start | bytes 100
  97.9 65.0 %copy-start.18 = (s32[8]{0:T(128)S(1)}, s32[8]{0:T(128)}, u32[]{:S(2)}) copy-start(s32[8]{0:T(128)} %constant.75.clone) | copy-start | bytes 100
  97.9 66.8 %copy-start.17 = (s32[8]{0:T(128)S(1)}, s32[8]{0:T(128)}, u32[]{:S(2)}) copy-start(s32[8]{0:T(128)} %constant.76.clone) | copy-start | bytes 100
  97.9 68.6 %copy-start.11 = (bf16[512]{0:T(512)(128)(2,1)S(1)}, bf16[512]{0:T(512)(128)(2,1)}, u32[]{:S(2)}) copy-start(bf16[512]{0:T(512)(128)(2,1)} %param.35) | copy-start | bytes 3076
  97.9 68.6 %copy-start.12 = (bf16[512]{0:T(512)(128)(2,1)S(1)}, bf16[512]{0:T(512)(128)(2,1)}, u32[]{:S(2)}) copy-start(bf16[512]{0:T(512)(128)(2,1)} %param.34) | copy-start | bytes 3076
  98.0 72.9 %copy-start.9 = (bf16[3,1408]{1,0:T(4,128)(2,1)S(1)}, bf16[3,1408]{1,0:T(4,128)(2,1)}, u32[]{:S(2)}) copy-start(bf16[3,1408]{1,0:T(4,128)(2,1)} %param.38) | copy-start | bytes 25348
  98.0 72.9 %copy-start.10 = (bf16[3,1408]{1,0:T(4,128)(2,1)S(1)}, bf16[3,1408]{1,0:T(4,128)(2,1)}, u32[]{:S(2)}) copy-start(bf16[3,1408]{1,0:T(4,128)(2,1)} %param.39) | copy-start | bytes 25348
  98.0 86.8 %all-to-all-start = ((bf16[4,384,512]{2,1,0:T(8,128)(2,1)}), bf16[4,384,512]{2,1,0:T(8,128)(2,1)S(1)}, u32[]{:S(2)}, u32[]{:S(2)}) async-start(bf16[4,384,512]{2,1,0:T(8,128)(2,1)} %pad_maximum_fusion), calls=%async_computation | async-start | bytes 3145728 | tf_op jit(solution)/shard_map/all_to_all | solution.py:122
  101.7 69.3 %collective-permute-start.10 = (bf16[1408,256]{1,0:T(8,128)(2,1)}, bf16[1408,256]{1,0:T(8,128)(2,1)}, u32[]{:S(2)}, u32[]{:S(2)}) collective-permute-start(bf16[1408,256]{1,0:T(8,128)(2,1)} %param.40), channel_id=1, source_target_pairs={{0,4},{8,0},{16,8},{24,16},{28,24},{20,28},{12,20},{4,12},{1,5},{9... | collective-permute-start | bytes 2162696 | tf_op jit(solution)/shard_map/ppermute | solution.py:60
  111.6 71.3 %collective-permute-start.7 = (bf16[1408,256]{1,0:T(8,128)(2,1)}, bf16[1408,256]{1,0:T(8,128)(2,1)}, u32[]{:S(2)}, u32[]{:S(2)}) collective-permute-start(bf16[1408,256]{1,0:T(8,128)(2,1)} %collective-permute-done.6), channel_id=1, source_target_pairs={{0,8},{8,16},{16,24},{24,28},{28,20},{20,12},{12,4},{4,0},{1,9},{9... | collective-permute-start | bytes 2162696 | tf_op jit(solution)/shard_map/ppermute | solution.py:60
  111.7 59.3 %collective-permute-start.4 = (s32[2]{0:T(128)S(1)}, s32[2]{0:T(128)S(1)}, u32[]{:S(2)}, u32[]{:S(2)}) collective-permute-start(s32[2]{0:T(128)S(1)} %slice.110), channel_id=1, source_target_pairs={{0,4},{4,8},{8,12},{12,16},{16,20},{20,24},{24,28},{1,5},{5,9},{9,... | collective-permute-start | bytes 32 | tf_op jit(solution)/shard_map/ppermute | solution.py:27
  171.0 94.5 %collective-permute-start.11 = (bf16[1408,256]{1,0:T(8,128)(2,1)}, bf16[1408,256]{1,0:T(8,128)(2,1)}, u32[]{:S(2)}, u32[]{:S(2)}) collective-permute-start(bf16[1408,256]{1,0:T(8,128)(2,1)} %collective-permute-done.10), channel_id=1, source_target_pairs={{0,4},{8,0},{16,8},{24,16},{28,24},{20,28},{12,20},{4,12},{1,5},{9... | collective-permute-start | bytes 2162696 | tf_op jit(solution)/shard_map/ppermute | solution.py:60
  182.9 85.6 %collective-permute-start.8 = (bf16[1408,256]{1,0:T(8,128)(2,1)}, bf16[1408,256]{1,0:T(8,128)(2,1)}, u32[]{:S(2)}, u32[]{:S(2)}) collective-permute-start(bf16[1408,256]{1,0:T(8,128)(2,1)} %collective-permute-done.7), channel_id=1, source_target_pairs={{0,8},{8,16},{16,24},{24,28},{28,20},{20,12},{12,4},{4,0},{1,9},{9... | collective-permute-start | bytes 2162696 | tf_op jit(solution)/shard_map/ppermute | solution.py:60
  193.5 18.9 %copy-start.3 = (bf16[384,512]{1,0:T(8,128)(2,1)}, bf16[384,512]{1,0:T(8,128)(2,1)S(1)}, u32[]{:S(2)}) copy-start(bf16[384,512]{1,0:T(8,128)(2,1)S(1)} %add_convert_fusion.1) | copy-start | bytes 1179652
  219.2 49.8 %collective-permute-start.5 = (bf16[2,1408]{1,0:T(2,128)(2,1)S(1)}, bf16[2,1408]{1,0:T(2,128)(2,1)S(1)}, u32[]{:S(2)}, u32[]{:S(2)}) collective-permute-start(bf16[2,1408]{1,0:T(2,128)(2,1)S(1)} %slice.138), channel_id=1, source_target_pairs={{0,4},{4,8},{8,12},{12,16},{16,20},{20,24},{24,28},{1,5},{5,9},{9,... | collective-permute-start | bytes 16904 | tf_op jit(solution)/shard_map/ppermute | solution.py:27
  262.2 6.7 %collective-permute-start.3 = (bf16[2,1408]{1,0:T(2,128)(2,1)S(1)}, bf16[2,1408]{1,0:T(2,128)(2,1)S(1)}, u32[]{:S(2)}, u32[]{:S(2)}) collective-permute-start(bf16[2,1408]{1,0:T(2,128)(2,1)S(1)} %slice.135), channel_id=1, source_target_pairs={{0,4},{4,8},{8,12},{12,16},{16,20},{20,24},{24,28},{1,5},{5,9},{9,... | collective-permute-start | bytes 16904 | tf_op jit(solution)/shard_map/ppermute | solution.py:27
  265.5 23.8 %collective-permute-start.12 = (bf16[1408,256]{1,0:T(8,128)(2,1)}, bf16[1408,256]{1,0:T(8,128)(2,1)S(1)}, u32[]{:S(2)}, u32[]{:S(2)}) collective-permute-start(bf16[1408,256]{1,0:T(8,128)(2,1)} %collective-permute-done.11), channel_id=1, source_target_pairs={{0,4},{8,0},{16,8},{24,16},{28,24},{20,28},{12,20},{4,12},{1,5},{9... | collective-permute-start | bytes 2162696 | tf_op jit(solution)/shard_map/ppermute | solution.py:60
  268.5 17.1 %collective-permute-start.9 = (bf16[1408,256]{1,0:T(8,128)(2,1)}, bf16[1408,256]{1,0:T(8,128)(2,1)S(1)}, u32[]{:S(2)}, u32[]{:S(2)}) collective-permute-start(bf16[1408,256]{1,0:T(8,128)(2,1)} %collective-permute-done.8), channel_id=1, source_target_pairs={{0,8},{8,16},{16,24},{24,28},{28,20},{20,12},{12,4},{4,0},{1,9},{9... | collective-permute-start | bytes 2162696 | tf_op jit(solution)/shard_map/ppermute | solution.py:60
  289.8 1.2 copy-start.2
  290.9 3.7 %copy-start.13 = (bf16[512]{0:T(512)(128)(2,1)S(1)}, bf16[512]{0:T(512)(128)(2,1)}, u32[]{:S(2)}) copy-start(bf16[512]{0:T(512)(128)(2,1)} %param.42) | copy-start | bytes 3076
  291.0 3.7 %copy-start.14 = (bf16[512]{0:T(512)(128)(2,1)S(1)}, bf16[512]{0:T(512)(128)(2,1)}, u32[]{:S(2)}) copy-start(bf16[512]{0:T(512)(128)(2,1)} %param.41) | copy-start | bytes 3076
  291.0 23.7 %all-to-all-start.1 = ((bf16[4,2,384,256]{3,2,1,0:T(8,128)(2,1)}), bf16[4,2,384,256]{3,2,1,0:T(8,128)(2,1)S(1)}, u32[]{:S(2)}, u32[]{:S(2)}) async-start(bf16[4,2,384,256]{3,2,1,0:T(8,128)(2,1)} %bitcast.79), calls=%async_computation.1 | async-start | bytes 3145728 | tf_op jit(solution)/shard_map/all_to_all | solution.py:261
  294.7 20.3 %copy-start.4 = (bf16[384,512]{1,0:T(8,128)(2,1)S(1)}, bf16[384,512]{1,0:T(8,128)(2,1)}, u32[]{:S(2)}) copy-start(bf16[384,512]{1,0:T(8,128)(2,1)} %copy-done.3) | copy-start | bytes 1179652
Sparse Core Ops, SparseCore 0:
  9.5 131.7 all-gather.4
  143.5 112.9 all-gather.2
